TPU v7x, 512 devices: a whole 4x8x8 slice. The times are simulated.
512 devices in a mesh: gr: 2 (over z_hi), fs: 32 (over z_lo, y), tp: 8 (over x, core).
Axes of the slice: x: 4, y: 8, z: 8 (z_hi: 2, z_lo: 4; z = z_hi * 4 + z_lo), core: 2. Of those that a mesh axis runs over, the one named last changes fastest.
Arguments:
- tokens: bfloat16 [16384, 2048], P(('gr', 'tp'), 'fs'), may hold values from -400 to 400
- norm_gain: float32 [2048], P('fs'), may hold values from 0.1 to 1.9
- up_weight: float32 [2048, 8192], P('fs', ('gr', 'tp')), may hold values from -0.125 to 0.125
- down_weight: float32 [8192, 2048], P('fs', ('gr', 'tp')), may hold values from -0.125 to 0.125
Outputs:
- mixed: bfloat16 [2048, 16384], P('fs', ('gr', 'tp'))
- up_ready: bfloat16 [2048, 8192], P(None, 'fs')
- down_ready: bfloat16 [8192, 2048], P('fs')
All inputs are finite; a program needn't handle non-finite values.
Results may differ from a plain program's by a relative error of at most 0.023.
Values may be sent and summed in bfloat16 or wider, within the bound.
A program may use at most 64 MiB of HBM per device.

v0:
```python
import jax
import jax.numpy as jnp
from jax import lax
from jax.sharding import Mesh
from jax.sharding import PartitionSpec as P

FS = ("fs_0", "fs_1")


epsilon = 1e-06


def laid_out(parts, dim):
    shape = list(parts.shape[1:])
    shape[dim] *= parts.shape[0]
    return jnp.moveaxis(parts, 0, dim).reshape(shape)


def gather_together(arrays, axis, dims):
    flat = jnp.concatenate([a.reshape(-1) for a in arrays])
    lines, at, done = (lax.all_gather(flat, axis), 0, [])
    for a, dim in zip(arrays, dims):
        parts = lines[:, at : at + a.size].reshape(-1, *a.shape)
        done.append(laid_out(parts, dim))
        at += a.size
    return tuple(done)


def gather_in_order(array, axes, sequence):
    parts = array[None]
    for k in sequence:
        parts = lax.all_gather(parts, axes[k], axis=0, tiled=True)
    current = [lax.axis_size(axes[k]) for k in reversed(sequence)]
    parts = parts.reshape(*current, *array.shape)
    turned = sorted(range(len(sequence)), key=lambda place: sequence[len(sequence) - 1 - place])
    return parts.transpose(*turned, *range(len(sequence), parts.ndim)).reshape(-1, *array.shape)


def whole_of(array, axes, sequence, dim):
    return laid_out(gather_in_order(array, axes, sequence), dim)


def own_block(parts, axes, sequence):
    inside = parts.shape[1:]
    parts = parts.reshape(*(lax.axis_size(a) for a in axes), *inside)
    parts = jnp.moveaxis(parts, sequence, range(len(axes))).reshape(-1, *inside)
    for k in sequence:
        parts = lax.psum_scatter(parts, axes[k], scatter_dimension=0, tiled=True)
    return parts[0]


def in_blocks(array, dim, length):
    shape = array.shape
    parts = array.reshape(*shape[:dim], length, shape[dim] // length, *shape[dim + 1 :])
    return jnp.moveaxis(parts, dim, 0)


def scatter_axes(array, axes, sequence, dim):
    length = lax.axis_size(axes)
    return own_block(in_blocks(array, dim, length), axes, sequence)


def shards(tokens, norm_gain, up_weight, down_weight):
    folded = (norm_gain[:, None] * up_weight).astype(jnp.bfloat16)
    down_cast = down_weight.astype(jnp.bfloat16)
    up_band, down_full = gather_together((folded, down_cast), ("gr", "tp"), (1, 1))
    up_full = lax.all_to_all(up_band, FS, split_axis=1, concat_axis=0, tiled=True)
    model_width = up_full.shape[0]
    piece = whole_of(tokens, FS, (0, 1), 1)
    running = jnp.dot(piece, up_full, preferred_element_type=jnp.float32)
    piece_wide = piece.astype(jnp.float32)
    squares = jnp.sum(piece_wide * piece_wide, axis=1)
    raw_up, squares = (running, squares)
    row_scale = lax.rsqrt(squares / model_width + epsilon)
    hidden = jnp.square(jax.nn.relu(raw_up * row_scale[:, None])).astype(jnp.bfloat16)
    outcome = (
        scatter_axes(
            lax.dot_general(
                down_full, hidden, (((0,), (1,)), ((), ())), preferred_element_type=jnp.float32
            ).astype(jnp.bfloat16),
            FS,
            (1, 0),
            0,
        )
        .astype(jnp.float32)
        .astype(jnp.bfloat16)
    )
    return (outcome, up_full, down_full)


def solution(mesh):
    split = Mesh(
        mesh.devices.reshape(mesh.shape["gr"], 4, 8, mesh.shape["tp"]), ("gr", "fs_0", "fs_1", "tp")
    )
    in_specs = (P(("gr", "tp"), FS), P(FS), P(FS, ("gr", "tp")), P(FS, ("gr", "tp")))
    out_specs = (P(FS, ("gr", "tp")), P(None, FS), P(FS, None))
    return jax.shard_map(
        shards, mesh=split, in_specs=in_specs, out_specs=out_specs, check_vma=False
    )
```

profile of v0, /device:TPU:6, one launch (start us, length us, event | category | flops | bytes accessed | tf_op | source)
XLA Modules:
  0.0 277.6 jit_solution(4540812072360673471)
XLA Ops:
  7.2 1.0 fusion.26
  8.2 0.9 convert_bitcast_fusion
  9.2 0.7 pad_maximum_fusion
  9.9 18.5 %all-gather.1 = bf16[4096,64]{0,1:T(8,128)(2,1)S(1)} all-gather(bf16[1024,64]{0,1:T(8,128)(2,1)} %param.4), channel_id=3, replica_groups=mesh['gr'=2,'fs_0'=4,'fs_1'=8,'tp'=8] {'fs_0'}, dimensions={0}, use_global_device_ids=true | all-gather | bytes 655360 | tf_op jit(solution)/shard_map/all_gather | solution.py:32
  28.4 0.9 copy.62
  29.3 55.5 %all-gather.7.cloned.1.call-done = bf16[1048576]{0:T(1024)(128)(2,1)} async-done(((bf16[65536]{0:T(1024)(128)(2,1)}), bf16[1048576]{0:T(1024)(128)(2,1)}) %all-gather.7.cloned.1.call-update) | async-done | bytes 2097168 | tf_op jit(solution)/shard_map/all_gather | solution.py:21
  84.8 2.1 reshape.50
  86.9 1.1 fusion.28
  88.4 0.6 copy.25
  89.0 0.4 all_to_all.14
  89.4 1.6 copy.26
  90.9 7.6 %all-to-all-start = ((bf16[64,32,256]{2,0,1:T(8,128)(2,1)}), bf16[64,32,256]{2,0,1:T(8,128)(2,1)S(1)}, u32[]{:S(2)}, u32[]{:S(2)}) async-start(bf16[64,32,256]{2,0,1:T(8,128)(2,1)} %copy.26), calls=%async_computation | async-start | bytes 2097152 | tf_op jit(solution)/shard_map/all_to_all | solution.py:67
  98.6 1.4 copy.37
  100.0 0.5 copy.24
  100.5 61.9 %all-gather.5.cloned.1.call-done = bf16[32,1024,64]{1,2,0:T(8,128)(2,1)} async-done(((bf16[4,1024,64]{1,2,0:T(8,128)(2,1)}), bf16[32,1024,64]{1,2,0:T(8,128)(2,1)}) %all-gather.5.cloned.1.call-update) | async-done | bytes 4194320 | tf_op jit(solution)/shard_map/all_gather | solution.py:32
  162.4 2.6 copy.29
  165.1 2.0 copy-done
  167.0 2.2 multiply_reduce_fusion
  169.2 8.8 %convolution_convert_fusion = bf16[2048,1024]{1,0:T(8,128)(2,1)} fusion(bf16[256,2048]{0,1:T(8,128)(2,1)S(1)} %bitcast.70, bf16[32,1024,64]{1,2,0:T(8,128)(2,1)} %bitcast.66, bf16[64,32,256]{2,0,1:T(8,128)(2,1)S(1)} %all-to-all-done, f32[1024]{0:T(1024)S(1)} %add_rsqrt_fusion), kind=kOutput, calls=%fused_computation.3 | convolution fusion | flops 2150629376 | bytes 10489856 | tf_op jit(solution)/shard_map/dot_general | solution.py:78
  178.0 4.9 %copy.31 = bf16[8,4,64,1024]{3,2,1,0:T(8,128)(2,1)} copy(bf16[8,4,64,1024]{3,2,0,1:T(8,128)(2,1)} %bitcast.68) | data formatting | bytes 8388608 | tf_op jit(solution)/shard_map/transpose | solution.py:46
  183.0 54.6 %reduce-scatter.3.cloned.1.call-done = bf16[4,64,1024]{2,1,0:T(8,128)(2,1)} async-done(((bf16[32,64,1024]{2,1,0:T(8,128)(2,1)}), bf16[4,64,1024]{2,1,0:T(8,128)(2,1)}) %reduce-scatter.3.cloned.1.call-update) | async-done | bytes 524304 | tf_op jit(solution)/shard_map/reduce_scatter | solution.py:48
  237.6 1.4 copy.33
  239.0 31.0 %reduce-scatter.5.cloned.1.call-done = bf16[1,64,1024]{2,1,0:T(8,128)(2,1)} async-done(((bf16[4,64,1024]{2,1,0:T(8,128)(2,1)}), bf16[1,64,1024]{2,1,0:T(8,128)(2,1)}) %reduce-scatter.5.cloned.1.call-update) | async-done | bytes 131088 | tf_op jit(solution)/shard_map/reduce_scatter | solution.py:48
  270.1 1.0 copy.64
  (13 shorter events, 0.6 us)
Async XLA Ops:
  7.2 77.6 %all-gather.7.cloned.1.call-start = ((), (), s32[]{:S(2)}) async-start(), calls=%async_computation.6 | async-start | bytes 2228224 | tf_op jit(solution)/shard_map/all_gather | solution.py:21
  9.8 152.6 %all-gather.5.cloned.1.call-start = ((), (), s32[]{:S(2)}) async-start(), calls=%async_computation.3 | async-start | bytes 4718592 | tf_op jit(solution)/shard_map/all_gather | solution.py:32
  90.9 78.3 %all-to-all-start = ((bf16[64,32,256]{2,0,1:T(8,128)(2,1)}), bf16[64,32,256]{2,0,1:T(8,128)(2,1)S(1)}, u32[]{:S(2)}, u32[]{:S(2)}) async-start(bf16[64,32,256]{2,0,1:T(8,128)(2,1)} %copy.26), calls=%async_computation | async-start | bytes 2097152 | tf_op jit(solution)/shard_map/all_to_all | solution.py:67
  98.5 139.1 %reduce-scatter.3.cloned.1.call-start = ((), (), s32[]{:S(2)}) async-start(), calls=%async_computation.4 | async-start | bytes 4718592 | tf_op jit(solution)/shard_map/reduce_scatter | solution.py:48
  165.1 2.0 copy-start
  182.9 87.2 %reduce-scatter.5.cloned.1.call-start = ((), (), s32[]{:S(2)}) async-start(), calls=%async_computation.5 | async-start | bytes 655360 | tf_op jit(solution)/shard_map/reduce_scatter | solution.py:48
Sparse Core Ops, SparseCore 0:
  11.9 72.8 all-gather.6
  86.9 75.4 all-gather.4
  183.0 54.5 reduce-scatter.2
  240.8 29.2 reduce-scatter.4
where the time goes:
time: 278 us
  waiting for transfers between devices  203 us (73%)
  local copies, waits for them, and re-layouts  20.8 us (7%)
  blocking collectives  18.5 us (7%)
  between operations  13.9 us (5%)
  matrix products  8.77 us (3%)
  starting transfers between devices  7.78 us (3%)
  other arithmetic  4.74 us (2%)
    reduce_scatter x2, waiting for transfers between devices, own_block(): parts = lax.psum_scatter(parts, axes[k], scatter_dimension=0, tiled=True)  85.7 us
    all_gather x1, waiting for transfers between devices, gather_in_order(): parts = lax.all_gather(parts, axes[k], axis=0, tiled=True)  61.9 us
    all_gather x1, waiting for transfers between devices, gather_together(): lines, at, done = (lax.all_gather(flat, axis), 0, [])  55.5 us
    all_gather x1, blocking collectives, gather_in_order(): parts = lax.all_gather(parts, axes[k], axis=0, tiled=True)  18.5 us
    dot_general x1, matrix products, shards(): lax.dot_general(down_full, hidden, (((0,), (1,)), ((), ())), preferred_el...  8.77 us
    all_to_all x1, starting transfers between devices, shards(): lax.all_to_all(up_band, FS, split_axis=1, concat_axis=0, tiled=True)  7.62 us
    unnamed x7, local copies, waits for them, and re-layouts  6.12 us
  transfers between devices with their start and end apart: 5, of which 4 were waited for; matrix products, arithmetic and copies ran while one was open for 5% of the time, Pallas kernels for 0%

commit v1 on v0

v1 whole, which is shorter than its diff:
```python
import functools

import jax
import jax.numpy as jnp
from jax import lax
from jax.experimental import pallas as pl
from jax.experimental.pallas import tpu as pltpu
from jax.sharding import Mesh
from jax.sharding import PartitionSpec as P

NZ, NY, NX, NC = 4, 8, 4, 2
AXES = ("gr", "z", "y", "x", "c")
MESH = pl.DeviceIdType.MESH
EPSILON = 1e-06
TN = (((0,), (0,)), ((), ()))


def kernel(
    x_ref, up_ref, dn_ref,
    mixed_ref, up_out, dn_out,
    upb, dnb, xg, raw, hid, part, rr, rl, zr,
    w_s, w_r, d_s, d_r, tz_s, tz_r, yr_s, yr_r, yl_s, yl_r,
    xu_s, xu_r, xd_s, xd_r, xf_s, xf_r, c_s, c_r, o_s,
    rr_s, rr_r, rl_s, rl_r, zz_s, zz_r,
):
    g, z, y, x, c = (lax.axis_index(a) for a in AXES)
    h = lax.rem(z, 2)
    zp = z + 1 - 2 * h
    right_y, left_y = lax.rem(y + 1, NY), lax.rem(y + NY - 1, NY)
    right_x, left_x = lax.rem(x + 1, NX), lax.rem(x + NX - 1, NX)
    far_x = lax.rem(x + 2, NX)
    mine = x * 2 + c
    other = 1 - c

    def remote(src, dst, send, recv, where):
        return pltpu.make_async_remote_copy(
            src_ref=src, dst_ref=dst, send_sem=send, recv_sem=recv, device_id=where, device_id_type=MESH
        )

    zt = g * 2 + x // 2
    targets = []
    for b in range(2):
        for gg in range(2):
            for p in range(2):
                tz = zt if p == 0 else zt + 1 - 2 * lax.rem(zt, 2)
                ty = lax.rem(x, 2) * 4 + c * 2 + b
                where = {"gr": gg, "z": tz, "y": ty, "x": z, "c": y // 4}
                same = (g == gg) & (z == tz) & (y == ty) & (x == z) & (c == y // 4)
                targets.append((b, gg, p, where, same))
    sources = []
    for p in range(2):
        zs = z if p == 0 else zp
        for j in range(4):
            sg, sx, sc = zs // 2, lax.rem(zs, 2) * 2 + y // 4, lax.rem(y // 2, 2)
            sy = c * 4 + j
            where = {"gr": sg, "z": x, "y": sy, "x": sx, "c": sc}
            same = (g == sg) & (z == x) & (y == sy) & (x == sx) & (c == sc)
            sources.append((p, j, where, same))

    near = [{"gr": 1 - g}, {"z": zp}, {"gr": 1 - g, "z": zp}, {"y": right_y}, {"y": left_y},
            {"x": right_x}, {"x": left_x}, {"c": other}]
    near += [{"z": lax.rem(z + k, NZ)} for k in range(1, NZ)]
    barrier = pltpu.get_barrier_semaphore()
    for where in near:
        pl.semaphore_signal(barrier, inc=1, device_id=where, device_id_type=MESH)
    for _, _, where, same in sources:
        @pl.when(jnp.logical_not(same))
        def _():
            pl.semaphore_signal(barrier, inc=1, device_id=where, device_id_type=MESH)
    expected = len(near)
    for _, _, _, _, same in targets:
        expected = expected + jnp.where(same, 0, 1)
    pl.semaphore_wait(barrier, expected)

    sent = []

    def go(copy):
        copy.start()
        sent.append(copy)
        return copy

    def half(of):
        return x_ref.at[:, pl.ds(pl.multiple_of(of * 512, 512), 512)]

    token_z = []
    for k in range(1, NZ):
        to = lax.rem(z + k, NZ)
        token_z.append(go(remote(half(lax.rem(to, 2)), xg.at[z, y], tz_s.at[k], tz_r.at[k], {"z": to})))

    def spread(s, j, side):
        zz = lax.rem(z + j, NZ)
        if side == "r":
            block, where, ss, rs = lax.rem(y + NY - s, NY), {"y": right_y}, yr_s, yr_r
        else:
            block, where, ss, rs = lax.rem(y + s, NY), {"y": left_y}, yl_s, yl_r
        if s == 3:
            at = xg.at[zz, block, pl.ds(0 if side == "r" else 32, 32)]
            return remote(at, at, ss.at[s, j], rs.at[s, j], where)
        src = half(h) if s == 0 and j == 0 else xg.at[zz, block]
        return remote(src, xg.at[zz, block], ss.at[s, j], rs.at[s, j], where)

    spread_r = {(s, j): spread(s, j, "r") for s in range(4) for j in range(4)}
    spread_l = {(s, j): spread(s, j, "l") for s in range(4) for j in range(4)}
    go(spread_r[0, 0])
    go(spread_l[0, 0])

    row = y * 64
    rows = pl.ds(pl.multiple_of(lax.rem(y, 4) * 64, 64), 64)
    place = z * 2 + y // 4
    up_copies = []
    for n, (b, gg, p, where, same) in enumerate(targets):
        piece = up_ref.at[:, pl.ds(b * 256, 256)]
        copy = remote(piece, upb.at[p, place, rows], w_s.at[n], w_r.at[p, lax.rem(y, 4)], where)
        up_copies.append((copy, same))

        @pl.when(jnp.logical_not(same))
        def _():
            copy.start()

        @pl.when(same)
        def _():
            upb[p, place, rows] = up_ref[:, b * 256 : (b + 1) * 256]

    down_copies = []
    for n, (where, p) in enumerate(
        [({"z": zp}, 1), ({"gr": 1 - g}, 0), ({"gr": 1 - g, "z": zp}, 1)]
    ):
        down_copies.append(go(remote(dn_ref, dnb.at[p, g, mine], d_s.at[n], d_r.at[n], where)))
    dnb[0, g, mine] = dn_ref[...]

    @pl.when(h == 0)
    def _():
        xg[z, y] = x_ref[:, :512]

    @pl.when(h == 1)
    def _():
        xg[z, y] = x_ref[:, 512:]

    for j in (3, 1, 2):
        token_z[NZ - j - 1].wait_recv()
        go(spread_r[0, j])
        go(spread_l[0, j])

    for p, j, where, same in sources:
        @pl.when(jnp.logical_not(same))
        def _():
            remote(
                up_ref.at[:, pl.ds(0, 256)], upb.at[p, mine, pl.ds(j * 64, 64)], w_s.at[0], w_r.at[p, j], where
            ).wait_recv()
    for copy in down_copies:
        copy.wait_recv()

    def to_core(which, at):
        if which == "u":
            n, ref = 0, upb.at[:, at * 2 + c]
        else:
            n, ref = 1, dnb.at[:, :, at * 2 + c]
        return ref, n

    def core_copy(which, at, k):
        ref, n = to_core(which, at)
        return go(remote(ref, ref, c_s.at[n, k], c_r.at[n, k], {"c": other}))

    up_own, dn_own = upb.at[:, mine], dnb.at[:, :, mine]
    xu_right = go(remote(up_own, up_own, xu_s.at[0], xu_r.at[0], {"x": right_x}))
    xu_left = go(remote(up_own, up_own, xu_s.at[1], xu_r.at[1], {"x": left_x}))
    core = [core_copy("u", x, 0), core_copy("d", x, 0)]
    xd_right = go(remote(dn_own, dn_own, xd_s.at[0], xd_r.at[0], {"x": right_x}))
    xd_left = go(remote(dn_own, dn_own, xd_s.at[1], xd_r.at[1], {"x": left_x}))

    def pass_on(s):
        for j in (0, 3, 1, 2):
            spread_r[s - 1, j].wait_recv()
            go(spread_r[s, j])
            spread_l[s - 1, j].wait_recv()
            go(spread_l[s, j])

    pass_on(1)
    xu_right.wait_recv()
    from_left = upb.at[:, left_x * 2 + c]
    xu_far = go(remote(from_left, from_left, xf_s.at[0], xf_r.at[0], {"x": right_x}))
    core.append(core_copy("u", left_x, 1))
    xu_left.wait_recv()
    core.append(core_copy("u", right_x, 2))
    pass_on(2)
    xd_left.wait_recv()
    from_right = dnb.at[:, :, right_x * 2 + c]
    xd_far = go(remote(from_right, from_right, xf_s.at[1], xf_r.at[1], {"x": left_x}))
    core.append(core_copy("d", right_x, 1))
    xd_right.wait_recv()
    core.append(core_copy("d", left_x, 2))
    pass_on(3)
    xu_far.wait_recv()
    core.append(core_copy("u", far_x, 3))
    xd_far.wait_recv()
    core.append(core_copy("d", far_x, 3))
    for j in range(4):
        spread_r[3, j].wait_recv()
        spread_l[3, j].wait_recv()
    for copy in core:
        copy.wait_recv()

    out_up = pltpu.make_async_copy(upb.at[0], up_out, o_s.at[0])
    out_dn = pltpu.make_async_copy(dnb.at[0], dn_out, o_s.at[1])
    out_up.start()
    out_dn.start()

    def accumulate(i, squares):
        block = xg[i // 2, pl.ds(lax.rem(i, 2) * 4, 4)].reshape(256, 512)
        for p in range(2):
            product = lax.dot_general(upb[p, i], block, TN, preferred_element_type=jnp.float32)

            @pl.when(i == 0)
            def _():
                raw[p] = product

            @pl.when(i > 0)
            def _():
                raw[p] += product
        wide = block.astype(jnp.float32)
        return squares + jnp.sum((wide * wide).reshape(32, 8, 512), axis=0)

    squares = lax.fori_loop(0, 8, accumulate, jnp.zeros((8, 512), jnp.float32))
    scale = lax.rsqrt(jnp.sum(squares, axis=0, keepdims=True) / 2048.0 + EPSILON)
    for p in range(2):
        hid[p] = jnp.square(jnp.maximum(raw[p] * scale, 0.0)).astype(jnp.bfloat16)

    def partial(i, carry):
        total = lax.dot_general(dnb[0, i // 8, lax.rem(i, 8)], hid[0], TN, preferred_element_type=jnp.float32)
        total += lax.dot_general(dnb[1, i // 8, lax.rem(i, 8)], hid[1], TN, preferred_element_type=jnp.float32)
        total = total.astype(jnp.bfloat16)
        at = lax.rem(i, 4) * 2
        part[at, i // 4] = total[:64]
        part[at + 1, i // 4] = total[64:]
        return carry

    lax.fori_loop(0, 16, partial, 0)

    def add_f32(a, b):
        return a.astype(jnp.float32) + b.astype(jnp.float32)

    moves_r, moves_l = {}, {}
    for s in range(4):
        to_r, to_l = lax.rem(y + 4 - s, NY), lax.rem(y + 4 + s, NY)
        for j in range(4):
            zz = lax.rem(z + 1 + j, NZ)
            if s == 1:
                moves_r[0, j].wait_recv()
                part[to_r, zz, :32] = add_f32(part[to_r, zz, :32], rr[0, j, :32]).astype(jnp.bfloat16)
                moves_l[0, j].wait_recv()
                part[to_l, zz, 32:] = add_f32(part[to_l, zz, 32:], rl[0, j, 32:]).astype(jnp.bfloat16)
            elif s > 1:
                moves_r[s - 1, j].wait_recv()
                part[to_r, zz] = add_f32(part[to_r, zz], rr[s - 1, j]).astype(jnp.bfloat16)
                moves_l[s - 1, j].wait_recv()
                part[to_l, zz] = add_f32(part[to_l, zz], rl[s - 1, j]).astype(jnp.bfloat16)
            rows_r, rows_l = (pl.ds(0, 32), pl.ds(32, 32)) if s == 0 else (pl.ds(0, 64),) * 2
            moves_r[s, j] = go(remote(
                part.at[to_r, zz, rows_r], rr.at[s, j, rows_r], rr_s.at[s, j], rr_r.at[s, j], {"y": right_y}))
            moves_l[s, j] = go(remote(
                part.at[to_l, zz, rows_l], rl.at[s, j, rows_l], rl_s.at[s, j], rl_r.at[s, j], {"y": left_y}))
    last = []
    for j in range(4):
        zz = lax.rem(z + 1 + j, NZ)
        moves_r[3, j].wait_recv()
        moves_l[3, j].wait_recv()
        total = add_f32(part[y, zz], rr[3, j]) + rl[3, j].astype(jnp.float32)
        if j < 3:
            part[y, zz] = total.astype(jnp.bfloat16)
            last.append(go(remote(part.at[y, zz], zr.at[j], zz_s.at[j], zz_r.at[j], {"z": zz})))
    for copy in last:
        copy.wait_recv()
    own = (total + zr[1].astype(jnp.float32)).astype(jnp.bfloat16)
    rest = add_f32(zr[0], zr[2]).astype(jnp.bfloat16)

    @pl.when(h == 0)
    def _():
        mixed_ref[:, :512] = own
        mixed_ref[:, 512:] = rest

    @pl.when(h == 1)
    def _():
        mixed_ref[:, 512:] = own
        mixed_ref[:, :512] = rest

    out_up.wait()
    out_dn.wait()
    for copy in sent:
        copy.wait_send()
    for copy, same in up_copies:
        @pl.when(jnp.logical_not(same))
        def _():
            copy.wait_send()


def layer(tokens_t, folded, down):
    dma = pltpu.SemaphoreType.DMA
    vmem = pl.BlockSpec(memory_space=pltpu.VMEM)
    hbm = pl.BlockSpec(memory_space=pl.ANY)
    bf16, f32 = jnp.bfloat16, jnp.float32
    return pl.pallas_call(
        kernel,
        out_shape=(
            jax.ShapeDtypeStruct((64, 1024), bf16),
            jax.ShapeDtypeStruct((8, 256, 256), bf16),
            jax.ShapeDtypeStruct((2, 8, 256, 128), bf16),
        ),
        in_specs=[vmem] * 3,
        out_specs=(vmem, hbm, hbm),
        scratch_shapes=[
            pltpu.VMEM((2, 8, 256, 256), bf16),
            pltpu.VMEM((2, 2, 8, 256, 128), bf16),
            pltpu.VMEM((4, 8, 64, 512), bf16),
            pltpu.VMEM((2, 256, 512), f32),
            pltpu.VMEM((2, 256, 512), bf16),
            pltpu.VMEM((8, 4, 64, 512), bf16),
            pltpu.VMEM((4, 4, 64, 512), bf16),
            pltpu.VMEM((4, 4, 64, 512), bf16),
            pltpu.VMEM((3, 64, 512), bf16),
            dma((8,)), dma((2, 4)), dma((3,)), dma((3,)), dma((4,)), dma((4,)),
            dma((4, 4)), dma((4, 4)), dma((4, 4)), dma((4, 4)),
            dma((2,)), dma((2,)), dma((2,)), dma((2,)), dma((2,)), dma((2,)),
            dma((2, 4)), dma((2, 4)), dma((2,)),
            dma((4, 4)), dma((4, 4)), dma((4, 4)), dma((4, 4)), dma((3,)), dma((3,)),
        ],
        compiler_params=pltpu.CompilerParams(
            collective_id=0, has_side_effects=True, vmem_limit_bytes=40 * 1024 * 1024
        ),
        name="ffn",
    )(tokens_t, folded, down)


def shards(tokens, norm_gain, up_weight, down_weight):
    folded = (norm_gain[:, None] * up_weight).astype(jnp.bfloat16)
    down = down_weight.astype(jnp.bfloat16)
    mixed, up_ready, down_ready = layer(tokens.T, folded, down)
    down_ready = down_ready.transpose(2, 0, 1, 3).reshape(256, 2048)
    return mixed, up_ready.reshape(2048, 256), down_ready


def solution(mesh):
    split = Mesh(mesh.devices.reshape(2, NZ, NY, NX, NC), AXES)
    groups, blocks = ("gr", "x", "c"), ("z", "y")
    in_specs = (P(groups, blocks), P(blocks), P(blocks, groups), P(blocks, groups))
    out_specs = (P(blocks, groups), P(None, blocks), P(blocks, None))
    return jax.shard_map(shards, mesh=split, in_specs=in_specs, out_specs=out_specs, check_vma=False)
```

time: 278 us -> 105 us (0.38)
  waiting for transfers between devices: 203 us -> 0 us
  Pallas kernels: 0 us -> 97.3 us
  blocking collectives: 18.5 us -> 0 us
  local copies, waits for them, and re-layouts: 20.8 us -> 4.47 us
  between operations: 13.9 us -> 0.69 us
  matrix products: 8.77 us -> 0 us
  starting transfers between devices: 7.78 us -> 0 us
  other arithmetic: 4.74 us -> 1.03 us
    all_gather x2 -> x0, waiting for transfers between devices: 117 us -> none  [the longest x1 61.9 us: gather_in_order(): parts = lax.all_gather(parts, axes[k], axis=0, tiled=True)]
    pallas_call x0 -> x1, Pallas kernels: none -> 97.3 us  [layer(): pl.pallas_call(kernel, out_shape=(jax.ShapeDtypeStruct((64, 1024), bf16),...]
    reduce_scatter x2 -> x0, waiting for transfers between devices: 85.7 us -> none  [own_block(): parts = lax.psum_scatter(parts, axes[k], scatter_dimension=0, tiled=True)]
    all_gather x1 -> x0, blocking collectives: 18.5 us -> none  [gather_in_order(): parts = lax.all_gather(parts, axes[k], axis=0, tiled=True)]
    dot_general x1 -> x0, matrix products: 8.77 us -> none  [shards(): lax.dot_general(down_full, hidden, (((0,), (1,)), ((), ())), preferred_el...]
    transpose x4 -> x1, local copies, waits for them, and re-layouts: 8.63 us -> 0.53 us  [shards(): down_ready = down_ready.transpose(2, 0, 1, 3).reshape(256, 2048)]
    all_to_all x1 -> x0, starting transfers between devices: 7.62 us -> none  [shards(): lax.all_to_all(up_band, FS, split_axis=1, concat_axis=0, tiled=True)]
    all_gather x2 -> x0, local copies, waits for them, and re-layouts: 2.99 us -> none  [the longest x1 2.14 us: gather_together(): lines, at, done = (lax.all_gather(flat, axis), 0, [])]
  transfers between devices with their start and end apart: 5 -> 0, of which waited for: 4 -> 0; matrix products, arithmetic and copies ran while one was open for 5% -> 0% of each run, Pallas kernels for 0% -> 0%
where the time goes in v1:
time: 105 us; the launch traced here: 103 us
  Pallas kernels  97.3 us (93%)
  local copies, waits for them, and re-layouts  4.47 us (4%)
    pallas_call x1, Pallas kernels, layer(): pl.pallas_call(kernel, out_shape=(jax.ShapeDtypeStruct((64, 1024), bf16),...  97.3 us
    unnamed x7, local copies, waits for them, and re-layouts  3.93 us

profile of v1, /device:TPU:6, one launch (start us, length us, event | category | flops | bytes accessed | tf_op | source)
XLA Modules:
  0.0 103.5 jit_solution(10222733425950852169)
XLA Ops:
  0.6 0.0 copy-start.1
  0.6 1.0 multiply_convert_fusion.up_ref
  1.7 0.0 copy-done.1
  1.7 0.0 copy-start
  1.7 0.9 copy-done
  2.6 97.3 %ffn.1 = (bf16[64,1024]{1,0:T(8,128)(2,1)S(1)}, bf16[8,256,256]{2,1,0:T(8,128)(2,1)S(1)}, bf16[2,8,256,128]{3,2,1,0:T(8,128)(2,1)S(1)}) custom-call(bf16[64,1024]{1,0:T(8,128)(2,1)S(1)} %bitcast.6, bf16[64,512]{1,0:T(8,128)(2,1)S(1)} %multiply_convert_fusion.up_ref, bf16[256,128]{1,0:T(8,128)(2,1)S(1)} %convert_element_type.7.dn_ref), custom_call_target="tpu_custom_call" | custom-call | tf_op jit(solution)/shard_map/ffn/pallas_call | solution.py:301
  99.9 0.5 copy.7
  100.4 1.4 %copy.8 = bf16[256,2048]{1,0:T(8,128)(2,1)} copy(bf16[256,2048]{0,1:T(8,128)(2,1)S(1)} %bitcast.7) | data formatting | bytes 2097152
  101.9 0.7 copy.11
  102.5 1.0 copy.12
  (1 shorter events, 0.0 us)
Async XLA Ops:
  0.6 1.0 %copy-start.1 = (f32[256,128]{1,0:T(8,128)S(1)}, f32[256,128]{1,0:T(8,128)}, u32[]{:S(2)}) copy-start(f32[256,128]{1,0:T(8,128)} %param.7) | copy-start | bytes 393220
  1.7 0.9 copy-start

commit v2 on v1

v2 whole, which is shorter than its diff:
```python
import functools

import jax
import jax.numpy as jnp
from jax import lax
from jax.experimental import pallas as pl
from jax.experimental.pallas import tpu as pltpu
from jax.sharding import Mesh
from jax.sharding import PartitionSpec as P

NZ, NY, NX, NC = 4, 8, 4, 2
AXES = ("gr", "z", "y", "x", "c")
MESH = pl.DeviceIdType.MESH
EPSILON = 1e-06
TN = (((0,), (0,)), ((), ()))


def kernel(
    x_hbm, gain_ref, up_hbm, dn_hbm,
    mixed_ref, up_out, dn_out,
    xs, uf, df, ub, db, upb, dnb, xg, raw, hid, part, rr, rl, zr,
    in_s, w_s, w_r, wp_s, wp_r, d_s, d_r, tz_s, tz_r, yr_s, yr_r, yl_s, yl_r,
    xu_s, xu_r, xd_s, xd_r, xf_s, xf_r, c_s, c_r,
    rr_s, rr_r, rl_s, rl_r, zz_s, zz_r,
):
    g, z, y, x, c = (lax.axis_index(a) for a in AXES)
    h = lax.rem(z, 2)
    zp = z + 1 - 2 * h
    right_y, left_y = lax.rem(y + 1, NY), lax.rem(y + NY - 1, NY)
    right_x, left_x = lax.rem(x + 1, NX), lax.rem(x + NX - 1, NX)
    far_x = lax.rem(x + 2, NX)
    mine = x * 2 + c
    other = 1 - c

    loads = [
        pltpu.make_async_copy(src, dst, in_s.at[n])
        for n, (src, dst) in enumerate(((x_hbm, xs), (up_hbm, uf), (dn_hbm, df)))
    ]
    for load in loads:
        load.start()

    def remote(src, dst, send, recv, where):
        return pltpu.make_async_remote_copy(
            src_ref=src, dst_ref=dst, send_sem=send, recv_sem=recv, device_id=where, device_id_type=MESH
        )

    inner = lax.rem((z + 1) // 2, 2)
    targets = []
    for b in range(2):
        for away in range(2):
            gg = g if away == 0 else 1 - g
            member = lax.rem(inner + g + away, 2)
            p = lax.rem(x // 2 + member, 2)
            tz = g * 2 + member
            ty = lax.rem(x, 2) * 4 + c * 2 + b
            where = {"gr": gg, "z": tz, "y": ty, "x": y // 2, "c": z // 2}
            same = (g == gg) & (z == tz) & (y == ty) & (x == y // 2) & (c == z // 2)
            targets.append((b, p, where, same))
    sg = z // 2
    class_of = lax.rem(z + sg + g + sg, 2)
    sz = class_of + c * (3 - 2 * class_of)
    sources = []
    for p in range(2):
        for j in range(2):
            sx, sy, sc = lax.rem(p + z, 2) * 2 + y // 4, x * 2 + j, lax.rem(y // 2, 2)
            where = {"gr": sg, "z": sz, "y": sy, "x": sx, "c": sc}
            same = (g == sg) & (z == sz) & (y == sy) & (x == sx) & (c == sc)
            sources.append((p, j, where, same))

    near = [{"gr": 1 - g, "z": zp}, {"y": right_y}, {"y": left_y}, {"x": right_x}, {"x": left_x}, {"c": other}]
    near += [{"z": lax.rem(z + k, NZ)} for k in range(1, NZ)]
    barrier = pltpu.get_barrier_semaphore()
    for _, _, where, same in sources:
        @pl.when(jnp.logical_not(same))
        def _():
            pl.semaphore_signal(barrier, inc=1, device_id=where, device_id_type=MESH)
    for where in near:
        pl.semaphore_signal(barrier, inc=1, device_id=where, device_id_type=MESH)
    expected = len(near)
    for _, _, _, same in targets:
        expected = expected + jnp.where(same, 0, 1)

    for load in loads:
        load.wait()
    eye = lax.broadcasted_iota(jnp.int32, (64, 64), 0) == lax.broadcasted_iota(jnp.int32, (64, 64), 1)
    column = jnp.sum(jnp.where(eye, gain_ref[...], 0.0), axis=1, keepdims=True)
    ub[...] = (column * uf[...]).astype(jnp.bfloat16)
    down_own = df[...].astype(jnp.bfloat16)
    db[...] = down_own
    dnb[0, g, mine] = down_own

    @pl.when(h == 0)
    def _():
        xg[z, y] = xs[:, :512]

    @pl.when(h == 1)
    def _():
        xg[z, y] = xs[:, 512:]

    pl.semaphore_wait(barrier, expected)

    sent = []

    def go(copy):
        copy.start()
        sent.append(copy)
        return copy

    def half(of):
        return xs.at[:, pl.ds(pl.multiple_of(of * 512, 512), 512)]

    token_z = []
    for k in range(1, NZ):
        to = lax.rem(z + k, NZ)
        token_z.append(go(remote(half(lax.rem(to, 2)), xg.at[z, y], tz_s.at[k], tz_r.at[k], {"z": to})))

    def spread(s, j, side):
        zz = lax.rem(z + j, NZ)
        if side == "r":
            block, where, ss, rs = lax.rem(y + NY - s, NY), {"y": right_y}, yr_s, yr_r
        else:
            block, where, ss, rs = lax.rem(y + s, NY), {"y": left_y}, yl_s, yl_r
        if s == 3:
            at = xg.at[zz, block, pl.ds(0 if side == "r" else 32, 32)]
            return remote(at, at, ss.at[s, j], rs.at[s, j], where)
        src = half(h) if s == 0 and j == 0 else xg.at[zz, block]
        return remote(src, xg.at[zz, block], ss.at[s, j], rs.at[s, j], where)

    spread_r = {(s, j): spread(s, j, "r") for s in range(4) for j in range(4)}
    spread_l = {(s, j): spread(s, j, "l") for s in range(4) for j in range(4)}

    def pass_on(s, *js):
        for j in js:
            if s > 0:
                spread_r[s - 1, j].wait_recv()
            go(spread_r[s, j])
            if s > 0:
                spread_l[s - 1, j].wait_recv()
            go(spread_l[s, j])

    pass_on(0, 0)

    offset = pl.multiple_of(lax.rem(z, 2) * 128 + lax.rem(y, 2) * 64, 64)
    place = (y // 2) * 2 + z // 2
    up_copies = []
    for n, (b, p, where, same) in enumerate(targets):
        piece = ub.at[:, pl.ds(b * 256, 256)]
        copy = remote(piece, upb.at[p, place, pl.ds(offset, 64)], w_s.at[n], w_r.at[p, lax.rem(y, 2)], where)
        up_copies.append((copy, same))

        @pl.when(jnp.logical_not(same))
        def _():
            copy.start()

        @pl.when(same)
        def _():
            upb[p, place, pl.ds(offset, 64)] = ub[:, b * 256 : (b + 1) * 256]

    dn_far = go(remote(db, dnb.at[1, g, mine], d_s.at[0], d_r.at[0], {"gr": 1 - g, "z": zp}))
    dn_near = go(remote(db, dnb.at[1, g, mine], d_s.at[1], d_r.at[1], {"z": zp}))

    def ring(send, recv, k, of):
        both = [go(remote(of(mine), of(mine), send.at[n, k], recv.at[n, k], {"x": to}))
                for n, to in enumerate((right_x, left_x))]
        return both

    def core_copy(ref, n, k):
        return go(remote(ref, ref, c_s.at[n, k], c_r.at[n, k], {"c": other}))

    def down_at(p, q):
        return lambda at: dnb.at[p, q, at]

    first = pl.multiple_of(lax.rem(sz, 2) * 128, 128)
    second = pl.multiple_of(128 - lax.rem(sz, 2) * 128, 128)

    def up_at(p, start):
        return lambda at: upb.at[p, at, pl.ds(start, 128)]

    downs = [down_at(0, g), down_at(1, g), down_at(1, 1 - g), down_at(0, 1 - g)]
    ups = [up_at(0, first), up_at(1, first), up_at(0, second), up_at(1, second)]
    xd = [[go(remote(db, downs[0](mine), xd_s.at[n, 0], xd_r.at[n, 0], {"x": to}))
           for n, to in enumerate((right_x, left_x))]]

    pass_on(1, 0)
    dn_near.wait_recv()
    xd.append(ring(xd_s, xd_r, 1, downs[1]))
    for j in (3, 1, 2):
        token_z[NZ - j - 1].wait_recv()
        pass_on(0, j)
    dn_far.wait_recv()
    dn_back = go(remote(dnb.at[1, 1 - g, mine], dnb.at[0, 1 - g, mine], d_s.at[2], d_r.at[2], {"z": zp}))
    xd.append(ring(xd_s, xd_r, 2, downs[2]))
    for p, j, where, same in sources:
        @pl.when(jnp.logical_not(same))
        def _():
            remote(
                ub.at[:, pl.ds(0, 256)], upb.at[p, mine, pl.ds(first + j * 64, 64)], w_s.at[0], w_r.at[p, j], where
            ).wait_recv()
    up_pair = [
        go(remote(ups[p](mine), ups[1 - p](mine), wp_s.at[p], wp_r.at[p], {"z": zp})) for p in range(2)
    ]
    xu = [ring(xu_s, xu_r, k, ups[k]) for k in range(2)]
    pass_on(1, 3, 1, 2)
    pass_on(2, 0)
    dn_back.wait_recv()
    xd.append(ring(xd_s, xd_r, 3, downs[3]))
    core_d = [core_copy(dnb.at[:, :, mine], 1, 0)]
    for copy in up_pair:
        copy.wait_recv()
    xu += [ring(xu_s, xu_r, k, ups[k]) for k in (2, 3)]
    core_u = [core_copy(upb.at[:, mine], 0, 0)]
    pass_on(2, 3, 1, 2)
    pass_on(3, 0)

    far_d = []
    for k in range(4):
        xd[k][1].wait_recv()
        at = downs[k](right_x * 2 + c)
        far_d.append(go(remote(at, at, xf_s.at[0, k], xf_r.at[0, k], {"x": left_x})))
        xd[k][0].wait_recv()
    core_d.append(core_copy(dnb.at[:, :, right_x * 2 + c], 1, 1))
    core_d.append(core_copy(dnb.at[:, :, left_x * 2 + c], 1, 2))
    far_u = []
    for k in range(4):
        xu[k][0].wait_recv()
        at = ups[k](left_x * 2 + c)
        far_u.append(go(remote(at, at, xf_s.at[1, k], xf_r.at[1, k], {"x": right_x})))
        xu[k][1].wait_recv()
    core_u.append(core_copy(upb.at[:, left_x * 2 + c], 0, 1))
    core_u.append(core_copy(upb.at[:, right_x * 2 + c], 0, 2))
    pass_on(3, 3, 1, 2)
    for copy in far_d:
        copy.wait_recv()
    core_d.append(core_copy(dnb.at[:, :, far_x * 2 + c], 1, 3))
    for copy in far_u:
        copy.wait_recv()
    core_u.append(core_copy(upb.at[:, far_x * 2 + c], 0, 3))
    for j in (0, 3, 1, 2):
        spread_r[3, j].wait_recv()
        spread_l[3, j].wait_recv()

    def tokens_of(at_x, at_c):
        return xg[pl.ds(at_c * 2, 2), pl.ds(at_x * 2, 2)].reshape(256, 512)

    def accumulate(at_x, at_c, first=False):
        for p in range(2):
            product = lax.dot_general(
                upb[p, at_x * 2 + at_c], tokens_of(at_x, at_c), TN, preferred_element_type=jnp.float32)
            if first:
                raw[p] = product
            else:
                raw[p] += product

    def square(i, squares):
        wide = tokens_of(i // 2, lax.rem(i, 2)).astype(jnp.float32)
        return squares + jnp.sum((wide * wide).reshape(32, 8, 512), axis=0)

    squares = lax.fori_loop(0, 8, square, jnp.zeros((8, 512), jnp.float32))
    scale = lax.rsqrt(jnp.sum(squares, axis=0, keepdims=True) / 2048.0 + EPSILON)

    for k, at in enumerate((x, left_x, right_x, far_x)):
        accumulate(at, c, first=k == 0)
    for k, at in enumerate((x, left_x, right_x, far_x)):
        core_u[k].wait_recv()
        accumulate(at, other)
    for p in range(2):
        hid[p] = jnp.square(jnp.maximum(raw[p] * scale, 0.0)).astype(jnp.bfloat16)
    for copy in core_d:
        copy.wait_recv()

    def pair_of(q):
        def one(zz, carry):
            hi, lo = zz // 2, lax.rem(zz, 2) * 4 + q
            total = lax.dot_general(dnb[0, hi, lo], hid[0], TN, preferred_element_type=jnp.float32)
            total += lax.dot_general(dnb[1, hi, lo], hid[1], TN, preferred_element_type=jnp.float32)
            total = total.astype(jnp.bfloat16)
            part[q * 2, zz] = total[:64]
            part[q * 2 + 1, zz] = total[64:]
            return carry

        lax.fori_loop(0, 4, one, 0)

    def add_f32(a, b):
        return a.astype(jnp.float32) + b.astype(jnp.float32)

    quarter = y // 2
    moves_r, moves_l = {}, {}
    pair_of(lax.rem(quarter + 2, 4))
    for s in range(4):
        to_r, to_l = lax.rem(y + 4 - s, NY), lax.rem(y + 4 + s, NY)
        for j in range(4):
            zz = lax.rem(z + 1 + j, NZ)
            if s == 1:
                moves_r[0, j].wait_recv()
                part[to_r, zz, :32] = add_f32(part[to_r, zz, :32], rr[0, j, :32]).astype(jnp.bfloat16)
                moves_l[0, j].wait_recv()
                part[to_l, zz, 32:] = add_f32(part[to_l, zz, 32:], rl[0, j, 32:]).astype(jnp.bfloat16)
            elif s > 1:
                moves_r[s - 1, j].wait_recv()
                part[to_r, zz] = add_f32(part[to_r, zz], rr[s - 1, j]).astype(jnp.bfloat16)
                moves_l[s - 1, j].wait_recv()
                part[to_l, zz] = add_f32(part[to_l, zz], rl[s - 1, j]).astype(jnp.bfloat16)
            rows_r, rows_l = (pl.ds(0, 32), pl.ds(32, 32)) if s == 0 else (pl.ds(0, 64),) * 2
            moves_r[s, j] = go(remote(
                part.at[to_r, zz, rows_r], rr.at[s, j, rows_r], rr_s.at[s, j], rr_r.at[s, j], {"y": right_y}))
            moves_l[s, j] = go(remote(
                part.at[to_l, zz, rows_l], rl.at[s, j, rows_l], rl_s.at[s, j], rl_r.at[s, j], {"y": left_y}))
        if s == 0:
            pair_of(lax.rem(quarter + 1, 4))
            pair_of(lax.rem(quarter + 3, 4))
        if s == 1:
            pair_of(quarter)
            for i in range(8):
                for zl in range(2):
                    to = ((i % 2 * 2 + zl) * 8 + i // 2 * 2) * 64
                    up_out[to : to + 128] = upb[0, i, zl * 128 : (zl + 1) * 128]
            for i in range(16):
                dn_out[:, i * 128 : (i + 1) * 128] = dnb[0, i // 8, i % 8]
    last = []
    for j in range(4):
        zz = lax.rem(z + 1 + j, NZ)
        moves_r[3, j].wait_recv()
        moves_l[3, j].wait_recv()
        total = add_f32(part[y, zz], rr[3, j]) + rl[3, j].astype(jnp.float32)
        if j < 3:
            part[y, zz] = total.astype(jnp.bfloat16)
            last.append(go(remote(part.at[y, zz], zr.at[j], zz_s.at[j], zz_r.at[j], {"z": zz})))
    for copy in last:
        copy.wait_recv()
    own = (total + zr[1].astype(jnp.float32)).astype(jnp.bfloat16)
    rest = add_f32(zr[0], zr[2]).astype(jnp.bfloat16)

    @pl.when(h == 0)
    def _():
        mixed_ref[:, :512] = own
        mixed_ref[:, 512:] = rest

    @pl.when(h == 1)
    def _():
        mixed_ref[:, 512:] = own
        mixed_ref[:, :512] = rest

    for copy in sent:
        copy.wait_send()
    for copy, same in up_copies:
        @pl.when(jnp.logical_not(same))
        def _():
            copy.wait_send()


def layer(tokens_t, gain, up, down):
    dma = pltpu.SemaphoreType.DMA
    vmem = pl.BlockSpec(memory_space=pltpu.VMEM)
    hbm = pl.BlockSpec(memory_space=pltpu.HBM)
    bf16, f32 = jnp.bfloat16, jnp.float32
    return pl.pallas_call(
        kernel,
        out_shape=(
            jax.ShapeDtypeStruct((64, 1024), bf16),
            jax.ShapeDtypeStruct((2048, 256), bf16),
            jax.ShapeDtypeStruct((256, 2048), bf16),
        ),
        in_specs=[hbm, vmem, hbm, hbm],
        out_specs=(vmem, vmem, vmem),
        scratch_shapes=[
            pltpu.VMEM((64, 1024), bf16),
            pltpu.VMEM((64, 512), f32),
            pltpu.VMEM((256, 128), f32),
            pltpu.VMEM((64, 512), bf16),
            pltpu.VMEM((256, 128), bf16),
            pltpu.VMEM((2, 8, 256, 256), bf16),
            pltpu.VMEM((2, 2, 8, 256, 128), bf16),
            pltpu.VMEM((4, 8, 64, 512), bf16),
            pltpu.VMEM((2, 256, 512), f32),
            pltpu.VMEM((2, 256, 512), bf16),
            pltpu.VMEM((8, 4, 64, 512), bf16),
            pltpu.VMEM((4, 4, 64, 512), bf16),
            pltpu.VMEM((4, 4, 64, 512), bf16),
            pltpu.VMEM((3, 64, 512), bf16),
            dma((3,)), dma((4,)), dma((2, 2)), dma((2,)), dma((2,)), dma((3,)), dma((3,)), dma((4,)), dma((4,)),
            dma((4, 4)), dma((4, 4)), dma((4, 4)), dma((4, 4)),
            dma((2, 4)), dma((2, 4)), dma((2, 4)), dma((2, 4)), dma((2, 4)), dma((2, 4)), dma((2, 4)), dma((2, 4)),
            dma((4, 4)), dma((4, 4)), dma((4, 4)), dma((4, 4)), dma((3,)), dma((3,)),
        ],
        compiler_params=pltpu.CompilerParams(
            collective_id=0, has_side_effects=True, vmem_limit_bytes=40 * 1024 * 1024
        ),
        name="ffn",
    )(tokens_t, gain, up, down)


def flush(*refs):
    sems = refs[-1]
    copies = [pltpu.make_async_copy(refs[n], refs[n + 3], sems.at[n]) for n in range(3)]
    for copy in copies:
        copy.start()
    for copy in copies:
        copy.wait()


def shards(tokens, norm_gain, up_weight, down_weight):
    def stay(a):
        return pltpu.with_memory_space_constraint(a, pltpu.HBM)

    results = layer(stay(tokens.T), norm_gain.reshape(1, 64), stay(up_weight), stay(down_weight))
    return pl.pallas_call(
        flush,
        out_shape=tuple(jax.ShapeDtypeStruct(r.shape, r.dtype) for r in results),
        in_specs=[pl.BlockSpec(memory_space=pltpu.VMEM)] * 3,
        out_specs=tuple([pl.BlockSpec(memory_space=pltpu.HBM)] * 3),
        scratch_shapes=[pltpu.SemaphoreType.DMA((3,))],
        compiler_params=pltpu.CompilerParams(vmem_limit_bytes=16 * 1024 * 1024),
        name="flush",
    )(*results)


def solution(mesh):
    split = Mesh(mesh.devices.reshape(2, NZ, NY, NX, NC), AXES)
    groups, blocks = ("gr", "x", "c"), ("z", "y")
    in_specs = (P(groups, blocks), P(blocks), P(blocks, groups), P(blocks, groups))
    out_specs = (P(blocks, groups), P(None, blocks), P(blocks, None))
    return jax.shard_map(shards, mesh=split, in_specs=in_specs, out_specs=out_specs, check_vma=False)
```

time: 105 us -> 80.7 us (0.77)
  the two profiles are of different devices: /device:TPU:6 before, /device:TPU:2 now
where the time goes in v2:
time: 80.7 us; the launch traced here: 80.6 us
  Pallas kernels  79.3 us (98%)
    pallas_call x1, Pallas kernels, layer(): pl.pallas_call(kernel, out_shape=(jax.ShapeDtypeStruct((64, 1024), bf16),...  77.9 us

profile of v2, /device:TPU:2, one launch (start us, length us, event | category | flops | bytes accessed | tf_op | source)
XLA Modules:
  0.0 80.6 jit_solution(4346096673028875694)
XLA Ops:
  0.6 0.0 copy-start
  0.6 0.6 copy-done
  1.3 77.9 %ffn.1 = (bf16[64,1024]{1,0:T(8,128)(2,1)S(1)}, bf16[2048,256]{1,0:T(8,128)(2,1)S(1)}, bf16[256,2048]{1,0:T(8,128)(2,1)S(1)}) custom-call(bf16[64,1024]{1,0:T(8,128)(2,1)} %bitcast.3, f32[1,64]{1,0:T(1,128)S(1)} %bitcast.2, f32[64,512]{1,0:T(8,128)} %up_hbm.1, f32[256,128]{1,0:T(8,128)} %dn_hbm.1), custom_call_target="tpu_custom_call" | custom-call | tf_op jit(solution)/shard_map/ffn/pallas_call | solution.py:356
  79.2 1.4 %flush.1 = (bf16[64,1024]{1,0:T(8,128)(2,1)}, bf16[2048,256]{1,0:T(8,128)(2,1)}, bf16[256,2048]{1,0:T(8,128)(2,1)}) custom-call(bf16[64,1024]{1,0:T(8,128)(2,1)S(1)} %get-tuple-element.6.refs_0_, bf16[2048,256]{1,0:T(8,128)(2,1)S(1)} %get-tuple-element.7.refs_1_, bf16[256,2048]{1,0:T(8,128)(2,1)S(1)} %get-tuple-element.8.refs_2_), custom_call_target="tpu_custom_call" | custom-call | tf_op jit(solution)/shard_map/flush/pallas_call | solution.py:406
Async XLA Ops:
  0.6 0.7 copy-start

commit v3 on v2

v3 whole, which is shorter than its diff:
```python
import functools

import jax
import jax.numpy as jnp
from jax import lax
from jax.experimental import pallas as pl
from jax.experimental.pallas import tpu as pltpu
from jax.sharding import Mesh
from jax.sharding import PartitionSpec as P

NZ, NY, NX, NC = 4, 8, 4, 2
EARLY = 16
AXES = ("gr", "z", "y", "x", "c")
MESH = pl.DeviceIdType.MESH
EPSILON = 1e-06
TN = (((0,), (0,)), ((), ()))


def kernel(
    x_hbm, gain_hbm, up_hbm, dn_hbm,
    mixed_ref, up_out, dn_out,
    xs, gf, uf, df, ub, db, upb, dnb, xg, raw, hid, part, rr, rl, zr,
    in_s, out_s, w_s, w_r, wp_r, d_r, tz_r, yr_r, yl_r, xu_r, xd_r, xf_r, c_r, rr_r, rl_r, zz_r,
):
    g, z, y, x, c = (lax.axis_index(a) for a in AXES)
    h = lax.rem(z, 2)
    zp = z + 1 - 2 * h
    right_y, left_y = lax.rem(y + 1, NY), lax.rem(y + NY - 1, NY)
    right_x, left_x = lax.rem(x + 1, NX), lax.rem(x + NX - 1, NX)
    far_x = lax.rem(x + 2, NX)
    mine = x * 2 + c
    other = 1 - c

    loads = [
        pltpu.make_async_copy(src, dst, in_s.at[n])
        for n, (src, dst) in enumerate(((x_hbm, xs), (gain_hbm, gf), (up_hbm, uf), (dn_hbm, df)))
    ]
    for load in loads:
        load.start()

    def remote(src, dst, send, recv, where):
        return pltpu.make_async_remote_copy(
            src_ref=src, dst_ref=dst, send_sem=send, recv_sem=recv, device_id=where, device_id_type=MESH
        )

    inner = lax.rem((z + 1) // 2, 2)
    targets = []
    for b in range(2):
        for away in range(2):
            gg = g if away == 0 else 1 - g
            member = lax.rem(inner + g + away, 2)
            p = lax.rem(x // 2 + member, 2)
            tz = g * 2 + member
            ty = lax.rem(x, 2) * 4 + c * 2 + b
            where = {"gr": gg, "z": tz, "y": ty, "x": y // 2, "c": z // 2}
            same = (g == gg) & (z == tz) & (y == ty) & (x == y // 2) & (c == z // 2)
            targets.append((b, p, where, same))
    sg = z // 2
    class_of = lax.rem(z + sg + g + sg, 2)
    sz = class_of + c * (3 - 2 * class_of)
    sources = []
    for p in range(2):
        for j in range(2):
            sx, sy, sc = lax.rem(p + z, 2) * 2 + y // 4, x * 2 + j, lax.rem(y // 2, 2)
            where = {"gr": sg, "z": sz, "y": sy, "x": sx, "c": sc}
            same = (g == sg) & (z == sz) & (y == sy) & (x == sx) & (c == sc)
            sources.append((p, j, where, same))

    near = [{"gr": 1 - g, "z": zp}, {"y": right_y}, {"y": left_y}, {"x": right_x}, {"x": left_x}, {"c": other}]
    near += [{"z": lax.rem(z + k, NZ)} for k in range(1, NZ)]
    barrier = pltpu.get_barrier_semaphore()
    for _, _, where, same in sources:
        @pl.when(jnp.logical_not(same))
        def _():
            pl.semaphore_signal(barrier, inc=1, device_id=where, device_id_type=MESH)
    for where in near:
        pl.semaphore_signal(barrier, inc=1, device_id=where, device_id_type=MESH)
    expected = len(near)
    for _, _, _, same in targets:
        expected = expected + jnp.where(same, 0, 1)

    for load in loads:
        load.wait()
    eye = lax.broadcasted_iota(jnp.int32, (64, 64), 0) == lax.broadcasted_iota(jnp.int32, (64, 64), 1)
    column = jnp.sum(jnp.where(eye, gf[...], 0.0), axis=1, keepdims=True)
    ub[...] = (column * uf[...]).astype(jnp.bfloat16)
    down_own = df[...].astype(jnp.bfloat16)
    db[...] = down_own
    dnb[0, g, mine] = down_own

    @pl.when(h == 0)
    def _():
        xg[z, y] = xs[:, :512]

    @pl.when(h == 1)
    def _():
        xg[z, y] = xs[:, 512:]

    pl.semaphore_wait(barrier, expected)

    def go(copy):
        copy.start()
        return copy

    S_CHAIN, S_FIRST, S_SIDE, S_PAIR, S_X, S_CORE, S_SUM, S_LAST = range(8)

    def half(of):
        return pl.ds(pl.multiple_of(of * 512, 512), 512)

    def spread(s, j, side):
        zz = lax.rem(z + j, NZ)
        if side == "r":
            block, where, rs = lax.rem(y + NY - s, NY), {"y": right_y}, yr_r
        else:
            block, where, rs = lax.rem(y + s, NY), {"y": left_y}, yl_r
        if s == 3:
            at = xg.at[zz, block, pl.ds(0, 32) if side == "r" else pl.ds(32, 32)]
            return remote(at, at, out_s.at[S_CHAIN], rs.at[s, j], where)
        at = xg.at[zz, block]
        src = xs.at[:, half(h)] if s == 0 and j == 0 else at
        return remote(src, at, out_s.at[S_CHAIN], rs.at[s, j], where)

    spread_r = {(s, j): spread(s, j, "r") for s in range(4) for j in range(4)}
    spread_l = {(s, j): spread(s, j, "l") for s in range(4) for j in range(4)}

    def pass_on(s, *js):
        for j in js:
            if s > 0:
                spread_r[s - 1, j].wait_recv()
            go(spread_r[s, j])
            if s > 0:
                spread_l[s - 1, j].wait_recv()
            go(spread_l[s, j])

    offset = pl.multiple_of(lax.rem(z, 2) * 128 + lax.rem(y, 2) * 64, 64)
    place = (y // 2) * 2 + z // 2
    up_copies = []
    for n, (b, p, where, same) in enumerate(targets):
        piece = ub.at[:, pl.ds(b * 256, 256)]
        copy = remote(piece, upb.at[p, place, pl.ds(offset, 64)], w_s.at[n], w_r.at[p, lax.rem(y, 2)], where)
        up_copies.append((copy, same))

        @pl.when(jnp.logical_not(same))
        def _():
            copy.start()

        @pl.when(same)
        def _():
            upb[p, place, pl.ds(offset, 64)] = ub[:, b * 256 : (b + 1) * 256]

    dn_far = go(remote(db, dnb.at[1, g, mine], out_s.at[S_SIDE], d_r.at[0], {"gr": 1 - g, "z": zp}))
    dn_near = go(remote(db, dnb.at[1, g, mine], out_s.at[S_SIDE], d_r.at[1], {"z": zp}))

    def ring(recv, k, of, src=None):
        at = of(mine)
        return [go(remote(at if src is None else src, at, out_s.at[S_X], recv.at[n, k], {"x": to}))
                for n, to in enumerate((right_x, left_x))]

    def core_copy(ref, n, k):
        return go(remote(ref, ref, out_s.at[S_CORE], c_r.at[n, k], {"c": other}))

    def down_at(p, q):
        return lambda at: dnb.at[p, q, at]

    first = pl.multiple_of(lax.rem(sz, 2) * 128, 128)
    second = pl.multiple_of(128 - lax.rem(sz, 2) * 128, 128)

    def up_at(p, start):
        return lambda at: upb.at[p, at, pl.ds(start, 128)]

    downs = [down_at(0, g), down_at(1, g), down_at(1, 1 - g), down_at(0, 1 - g)]
    ups = [up_at(0, first), up_at(1, first), up_at(0, second), up_at(1, second)]
    xd = [ring(xd_r, 0, downs[0], db)]

    pass_on(0, 0)
    token_z = []
    for k in range(1, NZ):
        to = lax.rem(z + k, NZ)
        token_z.append(go(remote(
            xs.at[:, half(lax.rem(to, 2))], xg.at[z, y],
            out_s.at[S_SIDE], tz_r.at[k - 1], {"z": to})))
    far = {}

    def forward(kind, pieces, at_of, k):
        for n in range(2):
            pieces[k][n].wait_recv()
        src, to = (left_x, right_x) if k % 2 == 0 else (right_x, left_x)
        at = at_of[k](src * 2 + c)
        far[kind, k] = go(remote(at, at, out_s.at[S_X], xf_r.at[kind, k], {"x": to}))

    dn_near.wait_recv()
    xd.append(ring(xd_r, 1, downs[1]))
    pass_on(1, 0)
    dn_far.wait_recv()
    dn_back = go(remote(
        dnb.at[1, 1 - g, mine], dnb.at[0, 1 - g, mine], out_s.at[S_SIDE], d_r.at[2], {"z": zp}))
    xd.append(ring(xd_r, 2, downs[2]))
    for j in (3, 1, 2):
        token_z[NZ - j - 1].wait_recv()
        pass_on(0, j)
    for p, j, where, same in sources:
        @pl.when(jnp.logical_not(same))
        def _():
            remote(
                ub.at[:, pl.ds(0, 256)], upb.at[p, mine, pl.ds(first + j * 64, 64)], w_s.at[0], w_r.at[p, j], where
            ).wait_recv()
    up_pair = [
        go(remote(ups[p](mine), ups[1 - p](mine), out_s.at[S_PAIR], wp_r.at[p], {"z": zp})) for p in range(2)
    ]
    xu = [ring(xu_r, k, ups[k]) for k in range(2)]
    forward(0, xd, downs, 0)
    forward(0, xd, downs, 1)
    pass_on(1, 3, 1, 2)
    pass_on(2, 0)
    dn_back.wait_recv()
    xd.append(ring(xd_r, 3, downs[3]))
    core_d = [core_copy(dnb.at[:, :, mine], 1, 0)]
    forward(0, xd, downs, 2)
    for copy in up_pair:
        copy.wait_recv()
    xu += [ring(xu_r, k, ups[k]) for k in (2, 3)]
    core_u = [core_copy(upb.at[:, mine], 0, 0)]
    forward(1, xu, ups, 0)
    forward(1, xu, ups, 1)
    pass_on(2, 3, 1, 2)
    pass_on(3, 0)
    forward(0, xd, downs, 3)
    core_d.append(core_copy(dnb.at[:, :, right_x * 2 + c], 1, 1))
    core_d.append(core_copy(dnb.at[:, :, left_x * 2 + c], 1, 2))
    forward(1, xu, ups, 2)
    forward(1, xu, ups, 3)
    core_u.append(core_copy(upb.at[:, left_x * 2 + c], 0, 1))
    core_u.append(core_copy(upb.at[:, right_x * 2 + c], 0, 2))
    pass_on(3, 3, 1, 2)
    for k in range(4):
        far[1, k].wait_recv()
    core_u.append(core_copy(upb.at[:, far_x * 2 + c], 0, 3))
    for k in range(4):
        far[0, k].wait_recv()
    core_d.append(core_copy(dnb.at[:, :, far_x * 2 + c], 1, 3))

    def tokens_of(at_x, at_c):
        return xg[pl.ds(at_c * 2, 2), pl.ds(at_x * 2, 2)].reshape(256, 512)

    def accumulate(at_x, at_c, first=False):
        for p in range(2):
            product = lax.dot_general(
                upb[p, at_x * 2 + at_c], tokens_of(at_x, at_c), TN, preferred_element_type=jnp.float32)
            if first:
                raw[p] = product
            else:
                raw[p] += product

    def square(at_x, at_c):
        wide = tokens_of(at_x, at_c).astype(jnp.float32)
        return jnp.sum((wide * wide).reshape(32, 8, 512), axis=0)

    quarter = y // 2
    late = lax.rem(quarter + 2, 4)
    for copy in core_u:
        copy.wait_recv()
    squares = jnp.zeros((8, 512), jnp.float32)
    for k in range(3):
        for at_c in range(2):
            at = lax.rem(late + 1 + k, 4)
            accumulate(at, at_c, first=k == 0 and at_c == 0)
            squares += square(at, at_c)
    for j in (0, 3, 1, 2):
        spread_r[3, j].wait_recv()
        spread_l[3, j].wait_recv()
    for at_c in range(2):
        accumulate(late, at_c)
        squares += square(late, at_c)
    scale = lax.rsqrt(jnp.sum(squares, axis=0, keepdims=True) / 2048.0 + EPSILON)
    for p in range(2):
        hid[p] = jnp.square(jnp.maximum(raw[p] * scale, 0.0)).astype(jnp.bfloat16)
    for copy in core_d:
        copy.wait_recv()

    def pair_of(q):
        total = 0.0
        for p in range(2):
            weights = jnp.concatenate([dnb[p, zz // 2, zz % 2 * 4 + q] for zz in range(4)], axis=1)
            total += lax.dot_general(weights, hid[p], TN, preferred_element_type=jnp.float32)
        total = total.astype(jnp.bfloat16)
        for zz in range(4):
            part[q * 2, zz] = total[zz * 128 : zz * 128 + 64]
            part[q * 2 + 1, zz] = total[zz * 128 + 64 : zz * 128 + 128]

    def add_f32(a, b):
        return a.astype(jnp.float32) + b.astype(jnp.float32)

    moves_r, moves_l = {}, {}

    def move(s, j):
        to_r, to_l, zz = lax.rem(y + 4 - s, NY), lax.rem(y + 4 + s, NY), lax.rem(z + 1 + j, NZ)
        if s > 0:
            moves_r[s - 1, j].wait_recv()
            rows = slice(0, 32) if s == 1 else slice(0, 64)
            part[to_r, zz, rows] = add_f32(part[to_r, zz, rows], rr[s - 1, j, rows]).astype(jnp.bfloat16)
        rows = pl.ds(0, 32) if s == 0 else pl.ds(0, 64)
        moves_r[s, j] = go(remote(
            part.at[to_r, zz, rows], rr.at[s, j, rows], out_s.at[S_SUM], rr_r.at[s, j], {"y": right_y}))
        if s > 0:
            moves_l[s - 1, j].wait_recv()
            rows = slice(32, 64) if s == 1 else slice(0, 64)
            part[to_l, zz, rows] = add_f32(part[to_l, zz, rows], rl[s - 1, j, rows]).astype(jnp.bfloat16)
        rows = pl.ds(32, 32) if s == 0 else pl.ds(0, 64)
        moves_l[s, j] = go(remote(
            part.at[to_l, zz, rows], rl.at[s, j, rows], out_s.at[S_SUM], rl_r.at[s, j], {"y": left_y}))

    pair_of(lax.rem(quarter + 2, 4))
    for j in range(4):
        move(0, j)
    pair_of(lax.rem(quarter + 1, 4))
    pair_of(lax.rem(quarter + 3, 4))
    for j in range(3):
        move(1, j)
    pair_of(quarter)
    for i in range(8):
        for zl in range(2):
            to = ((i % 2 * 2 + zl) * 8 + i // 2 * 2) * 64
            up_out[to : to + 128] = upb[0, i, zl * 128 : (zl + 1) * 128]
    for i in range(16):
        dn_out[:, i * 128 : (i + 1) * 128] = dnb[0, i // 8, i % 8]
    last = []

    def settle(j):
        zz = lax.rem(z + 1 + j, NZ)
        moves_r[3, j].wait_recv()
        moves_l[3, j].wait_recv()
        total = add_f32(part[y, zz], rr[3, j]) + rl[3, j].astype(jnp.float32)
        if j < 3:
            part[y, zz] = total.astype(jnp.bfloat16)
            last.append(go(remote(part.at[y, zz], zr.at[j], out_s.at[S_LAST], zz_r.at[j], {"z": zz})))
        return total

    for s, j in ((2, 0), (2, 1), (2, 2), (1, 3), (3, 0), (3, 1), (2, 3)):
        move(s, j)
    settle(0)
    move(3, 2)
    settle(1)
    move(3, 3)
    settle(2)
    total = settle(3)
    for copy in last:
        copy.wait_recv()
    own = (total + zr[1].astype(jnp.float32)).astype(jnp.bfloat16)
    rest = add_f32(zr[0], zr[2]).astype(jnp.bfloat16)

    @pl.when(h == 0)
    def _():
        mixed_ref[:, :512] = own
        mixed_ref[:, 512:] = rest

    @pl.when(h == 1)
    def _():
        mixed_ref[:, 512:] = own
        mixed_ref[:, :512] = rest

    for which, ref in (
        (S_CHAIN, part.at[pl.ds(0, 7)]),
        (S_SIDE, part.at[pl.ds(0, 2), pl.ds(0, 3)]),
        (S_PAIR, part.at[0, pl.ds(0, 2)]),
        (S_X, part.at[pl.ds(0, 6)]),
        (S_CORE, part),
        (S_SUM, part.at[pl.ds(0, 7)]),
        (S_LAST, part.at[0, pl.ds(0, 3)]),
    ):
        pltpu.make_async_copy(ref, ref, out_s.at[which]).wait()
    for copy, same in up_copies:
        @pl.when(jnp.logical_not(same))
        def _():
            copy.wait_send()


def layer(tokens_t, gain, up, down):
    dma = pltpu.SemaphoreType.DMA
    vmem = pl.BlockSpec(memory_space=pltpu.VMEM)
    hbm = pl.BlockSpec(memory_space=pltpu.HBM)
    bf16, f32 = jnp.bfloat16, jnp.float32
    return pl.pallas_call(
        kernel,
        out_shape=(
            jax.ShapeDtypeStruct((64, 1024), bf16),
            jax.ShapeDtypeStruct((2048, 256), bf16),
            jax.ShapeDtypeStruct((256, 2048), bf16),
        ),
        in_specs=[hbm] * 4,
        out_specs=(vmem, vmem, vmem),
        scratch_shapes=[
            pltpu.VMEM((64, 1024), bf16),
            pltpu.VMEM((1, 64), f32),
            pltpu.VMEM((64, 512), f32),
            pltpu.VMEM((256, 128), f32),
            pltpu.VMEM((64, 512), bf16),
            pltpu.VMEM((256, 128), bf16),
            pltpu.VMEM((2, 8, 256, 256), bf16),
            pltpu.VMEM((2, 2, 8, 256, 128), bf16),
            pltpu.VMEM((4, 8, 64, 512), bf16),
            pltpu.VMEM((2, 256, 512), f32),
            pltpu.VMEM((2, 256, 512), bf16),
            pltpu.VMEM((8, 4, 64, 512), bf16),
            pltpu.VMEM((4, 4, 64, 512), bf16),
            pltpu.VMEM((4, 4, 64, 512), bf16),
            pltpu.VMEM((3, 64, 512), bf16),
            dma((4,)), dma((8,)), dma((4,)), dma((2, 2)), dma((2,)), dma((3,)), dma((3,)),
            dma((4, 4)), dma((4, 4)), dma((2, 4)), dma((2, 4)), dma((2, 4)), dma((2, 4)),
            dma((4, 4)), dma((4, 4)), dma((3,)),
        ],
        compiler_params=pltpu.CompilerParams(
            collective_id=0, has_side_effects=True, vmem_limit_bytes=40 * 1024 * 1024
        ),
        name="ffn",
    )(tokens_t, gain, up, down)


def flush(*refs):
    sems = refs[-1]
    copies = [pltpu.make_async_copy(refs[n], refs[n + 3], sems.at[n]) for n in range(3)]
    for copy in copies:
        copy.start()
    for copy in copies:
        copy.wait()


def shards(tokens, norm_gain, up_weight, down_weight):
    def stay(a):
        return pltpu.with_memory_space_constraint(a, pltpu.HBM)

    results = layer(stay(tokens.T), stay(norm_gain.reshape(1, 64)), stay(up_weight), stay(down_weight))
    return pl.pallas_call(
        flush,
        out_shape=tuple(jax.ShapeDtypeStruct(r.shape, r.dtype) for r in results),
        in_specs=[pl.BlockSpec(memory_space=pltpu.VMEM)] * 3,
        out_specs=tuple([pl.BlockSpec(memory_space=pltpu.HBM)] * 3),
        scratch_shapes=[pltpu.SemaphoreType.DMA((3,))],
        compiler_params=pltpu.CompilerParams(vmem_limit_bytes=16 * 1024 * 1024),
        name="flush",
    )(*results)


def solution(mesh):
    split = Mesh(mesh.devices.reshape(2, NZ, NY, NX, NC), AXES)
    groups, blocks = ("gr", "x", "c"), ("z", "y")
    in_specs = (P(groups, blocks), P(blocks), P(blocks, groups), P(blocks, groups))
    out_specs = (P(blocks, groups), P(None, blocks), P(blocks, None))
    return jax.shard_map(shards, mesh=split, in_specs=in_specs, out_specs=out_specs, check_vma=False)
```

time: 80.7 us -> 78 us (0.967)
  the two profiles are of different devices: /device:TPU:2 before, /device:TPU:6 now
where the time goes in v3:
time: 78 us; the launch traced here: 77.5 us
  Pallas kernels  76.8 us (98%)
    pallas_call x1, Pallas kernels, layer(): pl.pallas_call(kernel, out_shape=(jax.ShapeDtypeStruct((64, 1024), bf16),...  75.5 us

profile of v3, /device:TPU:6, one launch (start us, length us, event | category | flops | bytes accessed | tf_op | source)
XLA Modules:
  0.0 77.5 jit_solution(15604927319987968548)
XLA Ops:
  0.6 75.5 %ffn.1 = (bf16[64,1024]{1,0:T(8,128)(2,1)S(1)}, bf16[2048,256]{1,0:T(8,128)(2,1)S(1)}, bf16[256,2048]{1,0:T(8,128)(2,1)S(1)}) custom-call(bf16[64,1024]{1,0:T(8,128)(2,1)} %bitcast.2, f32[1,64]{1,0:T(1,128)} %bitcast.3, f32[64,512]{1,0:T(8,128)} %up_hbm.1, f32[256,128]{1,0:T(8,128)} %dn_hbm.1), custom_call_target="tpu_custom_call" | custom-call | tf_op jit(solution)/shard_map/ffn/pallas_call | solution.py:382
  76.1 1.4 %flush.1 = (bf16[64,1024]{1,0:T(8,128)(2,1)}, bf16[2048,256]{1,0:T(8,128)(2,1)}, bf16[256,2048]{1,0:T(8,128)(2,1)}) custom-call(bf16[64,1024]{1,0:T(8,128)(2,1)S(1)} %get-tuple-element.6.refs_0_, bf16[2048,256]{1,0:T(8,128)(2,1)S(1)} %get-tuple-element.7.refs_1_, bf16[256,2048]{1,0:T(8,128)(2,1)S(1)} %get-tuple-element.8.refs_2_), custom_call_target="tpu_custom_call" | custom-call | tf_op jit(solution)/shard_map/flush/pallas_call | solution.py:432

commit v4 on v3

--- a/solution.py
+++ b/solution.py
@@ -9,7 +9,9 @@
 from jax.sharding import PartitionSpec as P
 
 NZ, NY, NX, NC = 4, 8, 4, 2
-EARLY = 16
+SIDES = (0, 1, -1, 2)
+SEQUENCE = "10 z3 z1 o1 o0 z2 n0 20 f0 13 11 u1 12 d0 p0 d1 30 b0 u0 U1 23 21 22 d2 q0 q1 q2 u3 33 31 32 d3 D0 D1 D2 U0"
+TAIL = "q3 U3 D3"
 AXES = ("gr", "z", "y", "x", "c")
 MESH = pl.DeviceIdType.MESH
 EPSILON = 1e-06
@@ -84,18 +86,7 @@
     eye = lax.broadcasted_iota(jnp.int32, (64, 64), 0) == lax.broadcasted_iota(jnp.int32, (64, 64), 1)
     column = jnp.sum(jnp.where(eye, gf[...], 0.0), axis=1, keepdims=True)
     ub[...] = (column * uf[...]).astype(jnp.bfloat16)
-    down_own = df[...].astype(jnp.bfloat16)
-    db[...] = down_own
-    dnb[0, g, mine] = down_own
-
-    @pl.when(h == 0)
-    def _():
-        xg[z, y] = xs[:, :512]
-
-    @pl.when(h == 1)
-    def _():
-        xg[z, y] = xs[:, 512:]
-
+    db[...] = df[...].astype(jnp.bfloat16)
     pl.semaphore_wait(barrier, expected)
 
     def go(copy):
@@ -148,16 +139,19 @@
         def _():
             upb[p, place, pl.ds(offset, 64)] = ub[:, b * 256 : (b + 1) * 256]
 
-    dn_far = go(remote(db, dnb.at[1, g, mine], out_s.at[S_SIDE], d_r.at[0], {"gr": 1 - g, "z": zp}))
-    dn_near = go(remote(db, dnb.at[1, g, mine], out_s.at[S_SIDE], d_r.at[1], {"z": zp}))
-
     def ring(recv, k, of, src=None):
         at = of(mine)
         return [go(remote(at if src is None else src, at, out_s.at[S_X], recv.at[n, k], {"x": to}))
                 for n, to in enumerate((right_x, left_x))]
 
-    def core_copy(ref, n, k):
-        return go(remote(ref, ref, out_s.at[S_CORE], c_r.at[n, k], {"c": other}))
+    def core_copy(kind, k, at_x):
+        n = SIDES.index(at_x)
+        at = (downs, ups)[kind][k](lax.rem(x + NX + at_x, NX) * 2 + c)
+        go(remote(at, at, out_s.at[S_CORE], c_r.at[kind, n], {"c": other}))
+
+    def from_core(kind, at_x):
+        at = dnb.at[:, :, mine] if kind == 0 else upb.at[:, mine]
+        pltpu.make_async_copy(at, at, c_r.at[kind, SIDES.index(at_x)]).wait()
 
     def down_at(p, q):
         return lambda at: dnb.at[p, q, at]
@@ -170,7 +164,6 @@
 
     downs = [down_at(0, g), down_at(1, g), down_at(1, 1 - g), down_at(0, 1 - g)]
     ups = [up_at(0, first), up_at(1, first), up_at(0, second), up_at(1, second)]
-    xd = [ring(xd_r, 0, downs[0], db)]
 
     pass_on(0, 0)
     token_z = []
@@ -179,65 +172,106 @@
         token_z.append(go(remote(
             xs.at[:, half(lax.rem(to, 2))], xg.at[z, y],
             out_s.at[S_SIDE], tz_r.at[k - 1], {"z": to})))
-    far = {}
-
-    def forward(kind, pieces, at_of, k):
-        for n in range(2):
-            pieces[k][n].wait_recv()
+    dn_far = go(remote(db, dnb.at[1, g, mine], out_s.at[S_SIDE], d_r.at[0], {"gr": 1 - g, "z": zp}))
+    dn_near = go(remote(db, dnb.at[1, g, mine], out_s.at[S_SIDE], d_r.at[1], {"z": zp}))
+    xd, xu = {0: ring(xd_r, 0, downs[0], db)}, {}
+
+    dnb[0, g, mine] = db[...]
+
+    @pl.when(h == 0)
+    def _():
+        xg[z, y] = xs[:, :512]
+
+    @pl.when(h == 1)
+    def _():
+        xg[z, y] = xs[:, 512:]
+
+    far, pair_sends = {}, {}
+
+    def to_pair(at_x):
+        at = lax.rem(x + NX + at_x, NX) * 2 + c
+        pair_sends[at_x] = go(remote(
+            ups[1](at), ups[0](at), out_s.at[S_PAIR], wp_r.at[SIDES.index(at_x)], {"z": zp}))
+
+    def forward(kind, k):
+        pieces, at_of = ((xd, downs), (xu, ups))[kind]
+        first_side = 0 if k % 2 == 0 else 1
+        pieces[k][first_side].wait_recv()
         src, to = (left_x, right_x) if k % 2 == 0 else (right_x, left_x)
         at = at_of[k](src * 2 + c)
         far[kind, k] = go(remote(at, at, out_s.at[S_X], xf_r.at[kind, k], {"x": to}))
-
-    dn_near.wait_recv()
-    xd.append(ring(xd_r, 1, downs[1]))
-    pass_on(1, 0)
-    dn_far.wait_recv()
-    dn_back = go(remote(
-        dnb.at[1, 1 - g, mine], dnb.at[0, 1 - g, mine], out_s.at[S_SIDE], d_r.at[2], {"z": zp}))
-    xd.append(ring(xd_r, 2, downs[2]))
-    for j in (3, 1, 2):
+        if (kind, k) == (1, 1):
+            to_pair(1)
+        core_copy(kind, k, -1 if k % 2 == 0 else 1)
+        pieces[k][1 - first_side].wait_recv()
+        if (kind, k) == (1, 1):
+            to_pair(-1)
+        core_copy(kind, k, 1 if k % 2 == 0 else -1)
+
+    def arrive(kind, k):
+        far[kind, k].wait_recv()
+        if (kind, k) == (1, 1):
+            to_pair(2)
+        core_copy(kind, k, 2)
+
+    core_copy(0, 0, 0)
+    late_sends = {}
+
+    def near_down():
+        dn_near.wait_recv()
+        xd[1] = ring(xd_r, 1, downs[1])
+        core_copy(0, 1, 0)
+
+    def far_down():
+        dn_far.wait_recv()
+        late_sends["back"] = go(remote(
+            dnb.at[1, 1 - g, mine], dnb.at[0, 1 - g, mine], out_s.at[S_SIDE], d_r.at[2], {"z": zp}))
+        xd[2] = ring(xd_r, 2, downs[2])
+        core_copy(0, 2, 0)
+
+    def back_down():
+        late_sends["back"].wait_recv()
+        xd[3] = ring(xd_r, 3, downs[3])
+        core_copy(0, 3, 0)
+
+    def own_up(p):
+        for k, j, where, same in sources:
+            if k == p:
+                @pl.when(jnp.logical_not(same))
+                def _():
+                    remote(
+                        ub.at[:, pl.ds(0, 256)], upb.at[p, mine, pl.ds(first + j * 64, 64)], w_s.at[0], w_r.at[p, j],
+                        where
+                    ).wait_recv()
+        if p == 0:
+            late_sends[0] = go(remote(ups[0](mine), ups[1](mine), out_s.at[S_PAIR], wp_r.at[4], {"z": zp}))
+        xu[p] = ring(xu_r, p, ups[p])
+        if p == 1:
+            to_pair(0)
+        core_copy(1, p, 0)
+
+    def pair_up(p):
+        late_sends[0].wait_recv()
+        xu[3] = ring(xu_r, 3, ups[3])
+        core_copy(1, 3, 0)
+
+    def from_pair(n):
+        at_x = SIDES[n]
+        pair_sends[at_x].wait_recv()
+        core_copy(1, 2, at_x)
+
+    def from_z(j):
         token_z[NZ - j - 1].wait_recv()
         pass_on(0, j)
-    for p, j, where, same in sources:
-        @pl.when(jnp.logical_not(same))
-        def _():
-            remote(
-                ub.at[:, pl.ds(0, 256)], upb.at[p, mine, pl.ds(first + j * 64, 64)], w_s.at[0], w_r.at[p, j], where
-            ).wait_recv()
-    up_pair = [
-        go(remote(ups[p](mine), ups[1 - p](mine), out_s.at[S_PAIR], wp_r.at[p], {"z": zp})) for p in range(2)
-    ]
-    xu = [ring(xu_r, k, ups[k]) for k in range(2)]
-    forward(0, xd, downs, 0)
-    forward(0, xd, downs, 1)
-    pass_on(1, 3, 1, 2)
-    pass_on(2, 0)
-    dn_back.wait_recv()
-    xd.append(ring(xd_r, 3, downs[3]))
-    core_d = [core_copy(dnb.at[:, :, mine], 1, 0)]
-    forward(0, xd, downs, 2)
-    for copy in up_pair:
-        copy.wait_recv()
-    xu += [ring(xu_r, k, ups[k]) for k in (2, 3)]
-    core_u = [core_copy(upb.at[:, mine], 0, 0)]
-    forward(1, xu, ups, 0)
-    forward(1, xu, ups, 1)
-    pass_on(2, 3, 1, 2)
-    pass_on(3, 0)
-    forward(0, xd, downs, 3)
-    core_d.append(core_copy(dnb.at[:, :, right_x * 2 + c], 1, 1))
-    core_d.append(core_copy(dnb.at[:, :, left_x * 2 + c], 1, 2))
-    forward(1, xu, ups, 2)
-    forward(1, xu, ups, 3)
-    core_u.append(core_copy(upb.at[:, left_x * 2 + c], 0, 1))
-    core_u.append(core_copy(upb.at[:, right_x * 2 + c], 0, 2))
-    pass_on(3, 3, 1, 2)
-    for k in range(4):
-        far[1, k].wait_recv()
-    core_u.append(core_copy(upb.at[:, far_x * 2 + c], 0, 3))
-    for k in range(4):
-        far[0, k].wait_recv()
-    core_d.append(core_copy(dnb.at[:, :, far_x * 2 + c], 1, 3))
+
+    steps = {
+        "n": lambda k: near_down(), "f": lambda k: far_down(), "b": lambda k: back_down(), "o": own_up, "p": pair_up,
+        "z": from_z, "q": from_pair, "d": lambda k: forward(0, k), "u": lambda k: forward(1, k),
+        "1": lambda j: pass_on(1, j), "2": lambda j: pass_on(2, j), "3": lambda j: pass_on(3, j),
+        "D": lambda k: arrive(0, k), "U": lambda k: arrive(1, k),
+    }
+    for step in SEQUENCE.split():
+        steps[step[0]](int(step[1]))
 
     def tokens_of(at_x, at_c):
         return xg[pl.ds(at_c * 2, 2), pl.ds(at_x * 2, 2)].reshape(256, 512)
@@ -257,25 +291,32 @@
 
     quarter = y // 2
     late = lax.rem(quarter + 2, 4)
-    for copy in core_u:
-        copy.wait_recv()
+    apart = lax.rem(late + NX - x, NX)
+    order = (
+        jnp.where(apart == 0, 1, 0), jnp.where(apart <= 1, 3, 1), jnp.where(apart == 2, 3, 2), apart
+    )
+
     squares = jnp.zeros((8, 512), jnp.float32)
-    for k in range(3):
+    for at_x in (0, -1, 1):
+        from_core(1, at_x)
+    for n in range(4):
+        if n == 2:
+            for step in TAIL.split():
+                steps[step[0]](int(step[1]))
+            from_core(1, 2)
+        if n == 3:
+            for j in (0, 3, 1, 2):
+                spread_r[3, j].wait_recv()
+                spread_l[3, j].wait_recv()
+        at = lax.rem(x + order[n], NX)
         for at_c in range(2):
-            at = lax.rem(late + 1 + k, 4)
-            accumulate(at, at_c, first=k == 0 and at_c == 0)
+            accumulate(at, at_c, first=n == 0 and at_c == 0)
             squares += square(at, at_c)
-    for j in (0, 3, 1, 2):
-        spread_r[3, j].wait_recv()
-        spread_l[3, j].wait_recv()
-    for at_c in range(2):
-        accumulate(late, at_c)
-        squares += square(late, at_c)
     scale = lax.rsqrt(jnp.sum(squares, axis=0, keepdims=True) / 2048.0 + EPSILON)
     for p in range(2):
         hid[p] = jnp.square(jnp.maximum(raw[p] * scale, 0.0)).astype(jnp.bfloat16)
-    for copy in core_d:
-        copy.wait_recv()
+    for at_x in SIDES:
+        from_core(0, at_x)
 
     def pair_of(q):
         total = 0.0
@@ -361,8 +402,8 @@
     for which, ref in (
         (S_CHAIN, part.at[pl.ds(0, 7)]),
         (S_SIDE, part.at[pl.ds(0, 2), pl.ds(0, 3)]),
-        (S_PAIR, part.at[0, pl.ds(0, 2)]),
-        (S_X, part.at[pl.ds(0, 6)]),
+        (S_PAIR, part.at[pl.ds(0, 5), 0]),
+        (S_X, part.at[pl.ds(0, 7), pl.ds(0, 3)]),
         (S_CORE, part),
         (S_SUM, part.at[pl.ds(0, 7)]),
         (S_LAST, part.at[0, pl.ds(0, 3)]),
@@ -404,7 +445,7 @@
             pltpu.VMEM((4, 4, 64, 512), bf16),
             pltpu.VMEM((4, 4, 64, 512), bf16),
             pltpu.VMEM((3, 64, 512), bf16),
-            dma((4,)), dma((8,)), dma((4,)), dma((2, 2)), dma((2,)), dma((3,)), dma((3,)),
+            dma((4,)), dma((8,)), dma((4,)), dma((2, 2)), dma((5,)), dma((3,)), dma((3,)),
             dma((4, 4)), dma((4, 4)), dma((2, 4)), dma((2, 4)), dma((2, 4)), dma((2, 4)),
             dma((4, 4)), dma((4, 4)), dma((3,)),
         ],
@@ -417,7 +458,12 @@
 
 def flush(*refs):
     sems = refs[-1]
-    copies = [pltpu.make_async_copy(refs[n], refs[n + 3], sems.at[n]) for n in range(3)]
+    copies = []
+    for n in range(3):
+        rows = refs[n].shape[0] // 4
+        for k in range(4):
+            at = pl.ds(k * rows, rows)
+            copies.append(pltpu.make_async_copy(refs[n].at[at], refs[n + 3].at[at], sems.at[n, k]))
     for copy in copies:
         copy.start()
     for copy in copies:
@@ -434,7 +480,7 @@
         out_shape=tuple(jax.ShapeDtypeStruct(r.shape, r.dtype) for r in results),
         in_specs=[pl.BlockSpec(memory_space=pltpu.VMEM)] * 3,
         out_specs=tuple([pl.BlockSpec(memory_space=pltpu.HBM)] * 3),
-        scratch_shapes=[pltpu.SemaphoreType.DMA((3,))],
+        scratch_shapes=[pltpu.SemaphoreType.DMA((3, 4))],
         compiler_params=pltpu.CompilerParams(vmem_limit_bytes=16 * 1024 * 1024),
         name="flush",
     )(*results)

time: 78 us -> 76.9 us (0.986)
  Pallas kernels: 76.8 us -> 75.7 us
    pallas_call x1, Pallas kernels: 75.5 us -> 74.3 us  [layer(): pl.pallas_call(kernel, out_shape=(jax.ShapeDtypeStruct((64, 1024), bf16),...]
where the time goes in v4:
time: 76.9 us; the launch traced here: 76.4 us
  Pallas kernels  75.7 us (98%)
    pallas_call x1, Pallas kernels, layer(): pl.pallas_call(kernel, out_shape=(jax.ShapeDtypeStruct((64, 1024), bf16),...  74.3 us

profile of v4, /device:TPU:6, one launch (start us, length us, event | category | flops | bytes accessed | tf_op | source)
XLA Modules:
  0.0 76.4 jit_solution(2085500667796375232)
XLA Ops:
  0.6 74.3 %ffn.1 = (bf16[64,1024]{1,0:T(8,128)(2,1)S(1)}, bf16[2048,256]{1,0:T(8,128)(2,1)S(1)}, bf16[256,2048]{1,0:T(8,128)(2,1)S(1)}) custom-call(bf16[64,1024]{1,0:T(8,128)(2,1)} %bitcast.2, f32[1,64]{1,0:T(1,128)} %bitcast.3, f32[64,512]{1,0:T(8,128)} %up_hbm.1, f32[256,128]{1,0:T(8,128)} %dn_hbm.1), custom_call_target="tpu_custom_call" | custom-call | tf_op jit(solution)/shard_map/ffn/pallas_call | solution.py:423
  74.9 1.5 %flush.1 = (bf16[64,1024]{1,0:T(8,128)(2,1)}, bf16[2048,256]{1,0:T(8,128)(2,1)}, bf16[256,2048]{1,0:T(8,128)(2,1)}) custom-call(bf16[64,1024]{1,0:T(8,128)(2,1)S(1)} %get-tuple-element.6.refs_0_, bf16[2048,256]{1,0:T(8,128)(2,1)S(1)} %get-tuple-element.7.refs_1_, bf16[256,2048]{1,0:T(8,128)(2,1)S(1)} %get-tuple-element.8.refs_2_), custom_call_target="tpu_custom_call" | custom-call | tf_op jit(solution)/shard_map/flush/pallas_call | solution.py:478

commit v5 on v4

--- a/solution.py
+++ b/solution.py
@@ -10,8 +10,11 @@
 
 NZ, NY, NX, NC = 4, 8, 4, 2
 SIDES = (0, 1, -1, 2)
-SEQUENCE = "10 z3 z1 o1 o0 z2 n0 20 f0 13 11 u1 12 d0 p0 d1 30 b0 u0 U1 23 21 22 d2 q0 q1 q2 u3 33 31 32 d3 D0 D1 D2 U0"
-TAIL = "q3 U3 D3"
+SEQUENCE = (
+    "10", "z3", "z1", "o1", "o0", "z2", "n0", "f0", "20", "13", "11", "u1", "12", "d0", "p0", "d1", "b0", "30", "u0",
+    "23", "U1", "d2", "21", "22", "d3", "q0", "q1", "q2", "u3", "33", "31", "32", "D0", "D1", "D2", "U0",
+)
+TAIL = ("q3", "U3", "D3")
 AXES = ("gr", "z", "y", "x", "c")
 MESH = pl.DeviceIdType.MESH
 EPSILON = 1e-06
@@ -270,7 +273,7 @@
         "1": lambda j: pass_on(1, j), "2": lambda j: pass_on(2, j), "3": lambda j: pass_on(3, j),
         "D": lambda k: arrive(0, k), "U": lambda k: arrive(1, k),
     }
-    for step in SEQUENCE.split():
+    for step in SEQUENCE:
         steps[step[0]](int(step[1]))
 
     def tokens_of(at_x, at_c):
@@ -301,7 +304,7 @@
         from_core(1, at_x)
     for n in range(4):
         if n == 2:
-            for step in TAIL.split():
+            for step in TAIL:
                 steps[step[0]](int(step[1]))
             from_core(1, 2)
         if n == 3:

time: 76.9 us -> 76.3 us (level)
  the two profiles are of different devices: /device:TPU:6 before, /device:TPU:66 now
where the time goes in v5:
time: 76.3 us; the launch traced here: 76.1 us
  Pallas kernels  75.5 us (99%)
    pallas_call x1, Pallas kernels, layer(): pl.pallas_call(kernel, out_shape=(jax.ShapeDtypeStruct((64, 1024), bf16),...  74 us

profile of v5, /device:TPU:66, one launch (start us, length us, event | category | flops | bytes accessed | tf_op | source)
XLA Modules:
  0.0 76.1 jit_solution(119104911414675849)
XLA Ops:
  0.6 74.0 %ffn.1 = (bf16[64,1024]{1,0:T(8,128)(2,1)S(1)}, bf16[2048,256]{1,0:T(8,128)(2,1)S(1)}, bf16[256,2048]{1,0:T(8,128)(2,1)S(1)}) custom-call(bf16[64,1024]{1,0:T(8,128)(2,1)} %bitcast.2, f32[1,64]{1,0:T(1,128)} %bitcast.3, f32[64,512]{1,0:T(8,128)} %up_hbm.1, f32[256,128]{1,0:T(8,128)} %dn_hbm.1), custom_call_target="tpu_custom_call" | custom-call | tf_op jit(solution)/shard_map/ffn/pallas_call | solution.py:426
  74.7 1.5 %flush.1 = (bf16[64,1024]{1,0:T(8,128)(2,1)}, bf16[2048,256]{1,0:T(8,128)(2,1)}, bf16[256,2048]{1,0:T(8,128)(2,1)}) custom-call(bf16[64,1024]{1,0:T(8,128)(2,1)S(1)} %get-tuple-element.6.refs_0_, bf16[2048,256]{1,0:T(8,128)(2,1)S(1)} %get-tuple-element.7.refs_1_, bf16[256,2048]{1,0:T(8,128)(2,1)S(1)} %get-tuple-element.8.refs_2_), custom_call_target="tpu_custom_call" | custom-call | tf_op jit(solution)/shard_map/flush/pallas_call | solution.py:481

commit v6 on v5

--- a/solution.py
+++ b/solution.py
@@ -14,7 +14,7 @@
     "10", "z3", "z1", "o1", "o0", "z2", "n0", "f0", "20", "13", "11", "u1", "12", "d0", "p0", "d1", "b0", "30", "u0",
     "23", "U1", "d2", "21", "22", "d3", "q0", "q1", "q2", "u3", "33", "31", "32", "D0", "D1", "D2", "U0",
 )
-TAIL = ("q3", "U3", "D3")
+TAIL = ("q3", "U3")
 AXES = ("gr", "z", "y", "x", "c")
 MESH = pl.DeviceIdType.MESH
 EPSILON = 1e-06
@@ -307,6 +307,7 @@
             for step in TAIL:
                 steps[step[0]](int(step[1]))
             from_core(1, 2)
+            arrive(0, 3)
         if n == 3:
             for j in (0, 3, 1, 2):
                 spread_r[3, j].wait_recv()

time: 76.3 us -> 76.8 us (level)
  the two profiles are of different devices: /device:TPU:66 before, /device:TPU:6 now
where the time goes in v6:
time: 76.8 us; the launch traced here: 75.6 us
  Pallas kernels  74.9 us (98%)
    pallas_call x1, Pallas kernels, layer(): pl.pallas_call(kernel, out_shape=(jax.ShapeDtypeStruct((64, 1024), bf16),...  73.5 us

profile of v6, /device:TPU:6, one launch (start us, length us, event | category | flops | bytes accessed | tf_op | source)
XLA Modules:
  0.0 75.6 jit_solution(13482489556187327648)
XLA Ops:
  0.6 73.5 %ffn.1 = (bf16[64,1024]{1,0:T(8,128)(2,1)S(1)}, bf16[2048,256]{1,0:T(8,128)(2,1)S(1)}, bf16[256,2048]{1,0:T(8,128)(2,1)S(1)}) custom-call(bf16[64,1024]{1,0:T(8,128)(2,1)} %bitcast.2, f32[1,64]{1,0:T(1,128)} %bitcast.3, f32[64,512]{1,0:T(8,128)} %up_hbm.1, f32[256,128]{1,0:T(8,128)} %dn_hbm.1), custom_call_target="tpu_custom_call" | custom-call | tf_op jit(solution)/shard_map/ffn/pallas_call | solution.py:427
  74.1 1.5 %flush.1 = (bf16[64,1024]{1,0:T(8,128)(2,1)}, bf16[2048,256]{1,0:T(8,128)(2,1)}, bf16[256,2048]{1,0:T(8,128)(2,1)}) custom-call(bf16[64,1024]{1,0:T(8,128)(2,1)S(1)} %get-tuple-element.6.refs_0_, bf16[2048,256]{1,0:T(8,128)(2,1)S(1)} %get-tuple-element.7.refs_1_, bf16[256,2048]{1,0:T(8,128)(2,1)S(1)} %get-tuple-element.8.refs_2_), custom_call_target="tpu_custom_call" | custom-call | tf_op jit(solution)/shard_map/flush/pallas_call | solution.py:482
